TPU v7x, 256 devices: a whole 4x4x8 slice. The times are simulated.
256 devices in a mesh: ep: 128 (over z, y, x), tp: 2 (over core).
Axes of the slice: x: 4, y: 4, z: 8, core: 2. Of those that a mesh axis runs over, the one named last changes fastest.
Arguments:
- tokens: bfloat16 [8192, 1024], P('ep', 'tp'), may hold values from -6 to 6
- norm_gain: float32 [1024], P('tp'), may hold values from 0.1 to 1.9
- routing: int32 [8192, 2], P('ep'), may hold values from 0 to 255, as said below
- route_weight: float32 [8192, 2], P('ep'), may hold values from 0.25 to 1
- w_gate: bfloat16 [256, 1024, 512], P('ep', None, 'tp'), may hold values from -0.1875 to 0.1875
- w_up: bfloat16 [256, 1024, 512], P('ep', None, 'tp'), may hold values from -0.1875 to 0.1875
- w_down: bfloat16 [256, 512, 1024], P('ep', None, 'tp'), may hold values from -0.25 to 0.25
Outputs:
- mixed: bfloat16 [8192, 1024], P('ep', 'tp')
Inputs may be any that keep to these rules, and one draw needn't show every extreme that they name: `routing`: each row names 2 different experts, all in the same group of 8 consecutive expert numbers. Among the rows of one device (aligned blocks of 64 rows) no expert is named more than 8 times, and in every block some expert is named exactly 8 times.
All inputs are finite; a program needn't handle non-finite values.
Results may differ from a plain program's by a relative error of at most 0.0015.
Values may be sent and summed in bfloat16 or wider, within the bound.
No kernel may reach another device: no remote copies, remote signals or barrier semaphores. Data moves between devices by JAX's collectives and lax.ppermute only.
A program may use at most 64 MiB of HBM per device.

v0:
```python
import functools

import jax
import jax.numpy as jnp
from jax import lax
from jax.experimental import pallas as pl
from jax.experimental.pallas import tpu as pltpu
from jax.sharding import Mesh, PartitionSpec as P


CAP = 8
EPS = 1e-06
INFO = 8
F32 = jnp.float32
BF16 = jnp.bfloat16
dot = functools.partial(jnp.dot, preferred_element_type=F32)


def iota(shape, dim):
    return lax.broadcasted_iota(jnp.int32, shape, dim)


def one_hot(mask):
    return mask.astype(F32).astype(BF16)


def parts(value):
    high = value.astype(BF16).astype(F32)
    middle = (value - high).astype(BF16).astype(F32)
    return [high, middle, value - high - middle]


def gather_kernel(own_ref, gain_ref, route_ref, weight_ref, out_ref):
    rows, half = own_ref.shape
    out_ref[0:rows, :] = own_ref[...]
    pad = jnp.zeros((5, half), F32)
    out_ref[rows:, :] = jnp.concatenate(
        [jnp.zeros((INFO, half), F32), *parts(gain_ref[...]), pad], axis=0
    ).astype(BF16)
    info = jnp.concatenate([route_ref[...].astype(F32), *parts(weight_ref[...])], axis=0)
    out_ref[rows : rows + INFO, 0:rows] = info.astype(BF16)


def norm_kernel(held_ref, other_ref, out_ref):
    rows, half = other_ref.shape
    own = held_ref[0:rows, :].astype(F32)
    other = other_ref[...].astype(F32)
    total = jnp.sum(own * own, axis=1, keepdims=True) + jnp.sum(other * other, axis=1, keepdims=True)
    scale = lax.rsqrt(total / (2 * half) + EPS)
    tail = held_ref[rows:, :]
    gain = tail[INFO:, :].astype(F32)
    gain = gain[0:1] + gain[1:2] + gain[2:3]
    out_ref[0:rows, :] = (own * scale * gain).astype(BF16)
    out_ref[rows:, :] = tail[0:INFO, :]


def dispatch_kernel(place_ref, own_ref, before_ref, opposite_ref, after_ref, out_ref, table0_ref, table1_ref):
    place_pair(0, place_ref, own_ref, before_ref, out_ref, table0_ref)
    place_pair(1, place_ref, opposite_ref, after_ref, out_ref, table1_ref)


def place_pair(pair, place_ref, a_ref, b_ref, out_ref, table_ref):
    rows = a_ref.shape[0] - INFO
    span = 2 * rows
    peers, block, half = out_ref.shape
    experts = 2 * peers
    earlier = one_hot(
        (iota((span, span), 0) < iota((span, span), 1))
        & (iota((span, span), 0) // rows == iota((span, span), 1) // rows)
    )
    side = iota((1, span), 1) // rows
    expert = iota((experts, span), 0)
    info = jnp.concatenate([a_ref[rows:, 0:rows].astype(F32), b_ref[rows:, 0:rows].astype(F32)], axis=1)
    tokens = jnp.concatenate([a_ref[0:rows, :], b_ref[0:rows, :]], axis=0)
    picks = [info[k : k + 1].astype(jnp.int32) - place_ref[0] // 2 * experts for k in range(2)]
    ahead = dot(one_hot((expert == picks[0]) | (expert == picks[1])), earlier)
    slots, weights = [], []
    for k, pick in enumerate(picks):
        rank = jnp.sum(jnp.where(expert == pick, ahead, 0.0), axis=0, keepdims=True).astype(jnp.int32)
        slot = (pick % 2) * (16 * peers) + (pick // 2) * 16 + side * CAP + rank
        slots.append(jnp.where((pick >= 0) & (pick < experts), slot, -1))
        weights.append(info[2 + k : 3 + k] + info[4 + k : 5 + k] + info[6 + k : 7 + k])
    for local in range(2):
        at = local * (block // 2) + 16 * pair
        slot = iota((16 * peers, span), 0) + local * 16 * peers
        sent = dot(one_hot((slot == slots[0]) | (slot == slots[1])), tokens)
        out_ref[:, at : at + 16, :] = sent.astype(BF16).reshape(peers, 16, half)
    columns = [slot.astype(F32) for slot in slots] + weights
    table_ref[...] = jnp.concatenate(columns + columns, axis=0).T


def hidden_part(rows_ref, at, gate_ref, up_ref, core):
    _, _, block, half = rows_ref.shape
    low, high = (rows_ref[at : at + 256 // block, side].reshape(256, half) for side in range(2))
    gate, up = (dot(low, ref[core, 0:half, :]) + dot(high, ref[core, half:, :]) for ref in (gate_ref, up_ref))
    return (gate / (1.0 + jnp.exp(-gate)) * up).astype(BF16)


def own_kernel(place_ref, rows_ref, gate_ref, up_ref, out_ref):
    chips, _, block, _ = rows_ref.shape
    for at in range(0, chips, 256 // block):
        out_ref[at * block : at * block + 256] = hidden_part(rows_ref, at, gate_ref, up_ref, place_ref[0] % 2)


def expert_kernel(place_ref, rows_ref, own_ref, gate2_ref, up2_ref, down_ref, down2_ref, out_ref):
    core = place_ref[0] % 2
    chips, _, block, half = rows_ref.shape
    width = own_ref.shape[1]
    sides = (core, 1 - core)
    spans = [pl.ds(pl.multiple_of(side * width, width), width) for side in sides]
    step = 256 // block
    for at in range(0, chips, step):
        own = own_ref[at * block : at * block + 256]
        other = hidden_part(rows_ref, at, gate2_ref, up2_ref, core)
        for side, down in zip(sides, (down_ref, down2_ref)):
            result = dot(own, down[core, spans[0], :]) + dot(other, down[core, spans[1], :])
            out_ref[at : at + step, side] = result.astype(BF16).reshape(step, block, half)


def combine_kernel(pair, back_ref, table_ref, a_ref, b_ref):
    rows, half = a_ref.shape
    peers, block, _ = back_ref.shape
    picked = [None, None]
    for local in range(2):
        at = local * (block // 2) + 16 * pair
        back = back_ref[:, at : at + 16, :].reshape(16 * peers, half)
        place = iota((2 * rows, 16 * peers), 1) + local * 16 * peers
        for k in range(2):
            term = dot(one_hot(place == table_ref[:, k : k + 1].astype(jnp.int32)), back)
            picked[k] = term if picked[k] is None else picked[k] + term
    total = (picked[0] * table_ref[:, 2:3] + picked[1] * table_ref[:, 3:4]).astype(BF16)
    a_ref[...] = total[0:rows]
    b_ref[...] = total[rows:]


def call(kernel, out_shape, args, flops, grant, scalars=0, **kw):
    moved = sum(a.size * a.dtype.itemsize for a in args)
    smem = pl.BlockSpec(memory_space=pltpu.SMEM)
    whole = pl.BlockSpec(memory_space=pltpu.VMEM)
    kw.setdefault("in_specs", [smem] * scalars + [whole] * (len(args) - scalars))
    return pl.pallas_call(
        kernel,
        out_shape=out_shape,
        cost_estimate=pl.CostEstimate(flops=flops, bytes_accessed=moved, transcendentals=0),
        compiler_params=pltpu.CompilerParams(vmem_limit_bytes=grant << 20),
        **kw,
    )(*args)


def local(tokens, norm_gain, routing, route_weight, w_gate, w_up, w_down):
    rows, half = tokens.shape
    columns = lax.axis_size("zh")
    plane = ("zl", "y", "x", "tp")
    peers = lax.axis_size(plane) // 2
    experts, _, width = w_gate.shape
    block = experts * columns * CAP
    total = peers * block
    place = (lax.axis_index("zh") * 2 + lax.axis_index("tp")).astype(jnp.int32).reshape(1)

    def swap(v):
        return lax.ppermute(v, "tp", [(0, 1), (1, 0)])

    def shift(v, by):
        return lax.ppermute(v, "zh", [(i, (i + by) % columns) for i in range(columns)])

    def exchange(v, axes):
        return lax.all_to_all(v, axes, split_axis=0, concat_axis=0, tiled=True)

    other = swap(tokens)
    gate2, up2, down2 = swap(w_gate), swap(w_up), swap(w_down)
    held = call(
        gather_kernel,
        jax.ShapeDtypeStruct((rows + INFO + 8, half), BF16),
        (tokens, norm_gain.reshape(1, half), routing.T, route_weight.T),
        rows * half,
        60,
    )
    own = call(norm_kernel, jax.ShapeDtypeStruct((rows + INFO, half), BF16), (held, other), rows * half, 4)
    opposite = shift(own, 2)
    before, after = shift(own, 1), shift(own, -1)

    buffer = jax.ShapeDtypeStruct((peers, block, half), BF16)
    small = jax.ShapeDtypeStruct((2 * rows, 8), F32)
    flops = total * 2 * rows * half
    sent, table0, table1 = call(
        dispatch_kernel, (buffer, small, small), (place, own, before, opposite, after), 2 * flops, 12, 1
    )
    arrived = exchange(sent.reshape(2 * peers, block // 2, half), plane)
    arrived = arrived.reshape(peers, 2, block // 2, half)
    hidden = call(
        own_kernel,
        jax.ShapeDtypeStruct((total // 2, width), BF16),
        (place, arrived, w_gate, w_up),
        total * half * width * 4,
        12,
        1,
    )
    result = call(
        expert_kernel,
        jax.ShapeDtypeStruct((peers, 2, block // 2, half), BF16),
        (place, arrived, hidden, gate2, up2, w_down, down2),
        total * half * width * 8,
        16,
        1,
    )
    back = exchange(result.reshape(2 * peers, block // 2, half), plane)
    back = back.reshape(peers, block, half)
    pair = (jax.ShapeDtypeStruct((rows, half), BF16),) * 2
    opposite, after = call(functools.partial(combine_kernel, 1), pair, (back, table1), 2 * flops, 8)
    own, before = call(functools.partial(combine_kernel, 0), pair, (back, table0), 2 * flops, 8)
    home = [shift(opposite, -2)]
    home += [shift(after, 1), shift(before, -1)]
    return sum((part.astype(F32) for part in home), own.astype(F32)).astype(BF16)


def solution(mesh):
    mesh = Mesh(mesh.devices.reshape(4, 2, 4, 4, 2), ("zh", "zl", "y", "x", "tp"))
    ep = ("zh", "zl", "y", "x")
    in_specs = (
        P(ep, "tp"),
        P("tp"),
        P(ep, None),
        P(ep, None),
        P(ep, None, "tp"),
        P(ep, None, "tp"),
        P(ep, None, "tp"),
    )

    return jax.shard_map(local, mesh=mesh, in_specs=in_specs, out_specs=P(ep, "tp"), check_vma=False)
```

profile of v0, /device:TPU:1, one launch (start us, length us, event | category | flops | bytes accessed | tf_op | source)
XLA Modules:
  0.0 115.3 jit_solution(16883338471753007460)
XLA Ops:
  0.0 3.2 %collective-permute-start = (bf16[64,512]{1,0:T(8,128)(2,1)}, bf16[64,512]{1,0:T(8,128)(2,1)S(1)}, u32[]{:S(2)}, u32[]{:S(2)}) collective-permute-start(bf16[64,512]{1,0:T(8,128)(2,1)} %own_ref.1), channel_id=1, source_target_pairs={{0,1},{1,0},{2,3},{3,2},{4,5},{5,4},{6,7},{7,6},{8,9},{9,8},{10,11... | collective-permute-start | bytes 196616 | tf_op jit(solution)/shard_map/ppermute | solution.py:161
  3.2 1.5 %shard_map.73.held_ref = bf16[80,512]{1,0:T(8,128)(2,1)} custom-call(bf16[64,512]{1,0:T(8,128)(2,1)} %own_ref.1, f32[1,512]{1,0:T(1,128)} %bitcast.14, s32[2,64]{1,0:T(2,128)} %bitcast.15, f32[2,64]{1,0:T(2,128)} %bitcast.16), custom_call_target="tpu_custom_call" | custom-call | flops 32768 | bytes 68608 | tf_op jit(solution)/shard_map/pallas_call | solution.py:141
  4.7 0.0 collective-permute-done.other_ref
  4.7 0.0 copy-start.4
  4.7 0.9 copy-done.4
  5.6 0.1 shard_map.74.own_ref
  5.7 4.4 %collective-permute-start.3 = (bf16[72,512]{1,0:T(8,128)(2,1)S(1)}, bf16[72,512]{1,0:T(8,128)(2,1)S(1)}, u32[]{:S(2)}, u32[]{:S(2)}) collective-permute-start(bf16[72,512]{1,0:T(8,128)(2,1)S(1)} %shard_map.74.own_ref), channel_id=1, source_target_pairs={{0,192},{64,0},{128,64},{192,128},{1,193},{65,1},{129,65},{193,129... | collective-permute-start | bytes 221192 | tf_op jit(solution)/shard_map/ppermute | solution.py:164
  10.1 1.0 collective-permute-start.2
  11.1 2.3 %collective-permute-start.1 = (bf16[72,512]{1,0:T(8,128)(2,1)S(1)}, bf16[72,512]{1,0:T(8,128)(2,1)S(1)}, u32[]{:S(2)}, u32[]{:S(2)}) collective-permute-start(bf16[72,512]{1,0:T(8,128)(2,1)S(1)} %shard_map.74.own_ref), channel_id=1, source_target_pairs={{0,64},{64,128},{128,192},{192,0},{1,65},{65,129},{129,193},{193,1... | collective-permute-start | bytes 221192 | tf_op jit(solution)/shard_map/ppermute | solution.py:164
  13.4 0.0 collective-permute-done.3.after_ref
  13.4 4.2 %collective-permute-done.2.opposite_ref = bf16[72,512]{1,0:T(8,128)(2,1)S(1)} collective-permute-done((bf16[72,512]{1,0:T(8,128)(2,1)S(1)}, bf16[72,512]{1,0:T(8,128)(2,1)S(1)}, u32[]{:S(2)}, u32[]{:S(2)}) %collective-permute-start.2) | collective-permute-done | bytes 73760 | tf_op jit(solution)/shard_map/ppermute | solution.py:164
  17.6 0.9 collective-permute-done.1.before_ref
  18.5 1.0 shard_map.75
  19.5 0.0 copy-start
  19.5 1.3 %copy-done = bf16[32,64,512]{2,1,0:T(8,128)(2,1)} copy-done((bf16[32,64,512]{2,1,0:T(8,128)(2,1)}, bf16[32,64,512]{2,1,0:T(8,128)(2,1)S(1)}, u32[]{:S(2)}) %copy-start) | copy-done | bytes 2097176
  20.9 0.0 copy-start.1
  20.9 10.6 %all-to-all-start = ((bf16[64,32,512]{2,1,0:T(8,128)(2,1)}), bf16[64,32,512]{2,1,0:T(8,128)(2,1)S(1)}, u32[]{:S(2)}, u32[]{:S(2)}) async-start(bf16[64,32,512]{2,1,0:T(8,128)(2,1)} %bitcast.13), calls=%async_computation | async-start | bytes 4194304 | tf_op jit(solution)/shard_map/all_to_all | solution.py:167
  31.5 0.0 copy-done.1
  31.5 0.5 collective-permute-start.4
  32.0 0.1 collective-permute-start.5
  32.1 0.4 collective-permute-start.6
  32.5 26.5 %all-to-all-done = bf16[64,32,512]{2,1,0:T(8,128)(2,1)S(1)} async-done(((bf16[64,32,512]{2,1,0:T(8,128)(2,1)}), bf16[64,32,512]{2,1,0:T(8,128)(2,1)S(1)}, u32[]{:S(2)}, u32[]{:S(2)}) %all-to-all-start) | async-done | bytes 2097184 | tf_op jit(solution)/shard_map/all_to_all | solution.py:167
  59.0 0.0 copy-start.2
  59.0 1.2 %copy-done.2 = bf16[2,1024,256]{2,1,0:T(8,128)(2,1)S(1)} copy-done((bf16[2,1024,256]{2,1,0:T(8,128)(2,1)S(1)}, bf16[2,1024,256]{2,1,0:T(8,128)(2,1)}, u32[]{:S(2)}) %copy-start.2) | copy-done | bytes 1048600
  60.2 0.0 copy-start.3
  60.2 1.3 %shard_map.76.own_ref = bf16[1024,256]{1,0:T(8,128)(2,1)S(1)} custom-call(s32[1]{0:T(128)} %bitcast.place_ref, bf16[32,2,32,512]{3,2,1,0:T(8,128)(2,1)S(1)} %bitcast.8, bf16[2,1024,256]{2,1,0:T(8,128)(2,1)S(1)} %copy-done.1, bf16[2,1024,256]{2,1,0:T(8,128)(2,1)S(1)} %copy-done.2), custom_call_target="tpu_custom_call" | custom-call | flops 1073741824 | bytes 4194308 | tf_op jit(solution)/shard_map/pallas_call | solution.py:141
  61.5 0.0 collective-permute-done.4.gate2_ref
  61.5 0.0 collective-permute-done.5.up2_ref
  61.5 0.0 collective-permute-done.6.down2_ref
  61.5 0.0 copy-done.3
  61.6 4.6 %shard_map.77 = bf16[32,2,32,512]{3,2,1,0:T(8,128)(2,1)S(1)} custom-call(s32[1]{0:T(128)} %bitcast.place_ref, bf16[32,2,32,512]{3,2,1,0:T(8,128)(2,1)S(1)} %bitcast.9, bf16[1024,256]{1,0:T(8,128)(2,1)S(1)} %shard_map.76.own_ref, bf16[2,1024,256]{2,1,0:T(8,128)(2,1)} %collective-permute-done.4.gate2_ref, ...), custom_call_target="tpu_custom_call" | custom-call | flops 2147483648 | bytes 6815748 | tf_op jit(solution)/shard_map/pallas_call | solution.py:141
  66.2 34.8 %all_to_all.10 = bf16[64,32,512]{2,1,0:T(8,128)(2,1)S(1)} all-to-all(bf16[64,32,512]{2,1,0:T(8,128)(2,1)S(1)} %bitcast.12), channel_id=1, replica_groups=mesh['zh'=4,'zl'=2,'y'=4,'x'=4,'tp'=2] {'zl','y','x','tp'}, dimensions={0} | all-to-all | bytes 4194304 | tf_op jit(solution)/shard_map/all_to_all | solution.py:167
  101.0 0.5 shard_map.79
  101.5 0.5 shard_map.78
  102.0 4.2 %collective-permute-start.7 = (bf16[64,512]{1,0:T(8,128)(2,1)S(1)}, bf16[64,512]{1,0:T(8,128)(2,1)S(1)}, u32[]{:S(2)}, u32[]{:S(2)}) collective-permute-start(bf16[64,512]{1,0:T(8,128)(2,1)S(1)} %get-tuple-element.16), channel_id=1, source_target_pairs={{0,128},{64,192},{128,0},{192,64},{1,129},{65,193},{129,1},{193,65... | collective-permute-start | bytes 196616 | tf_op jit(solution)/shard_map/ppermute | solution.py:164
  106.2 0.8 collective-permute-start.8
  107.0 2.8 %collective-permute-start.9 = (bf16[64,512]{1,0:T(8,128)(2,1)S(1)}, bf16[64,512]{1,0:T(8,128)(2,1)S(1)}, u32[]{:S(2)}, u32[]{:S(2)}) collective-permute-start(bf16[64,512]{1,0:T(8,128)(2,1)S(1)} %get-tuple-element.18), channel_id=1, source_target_pairs={{0,192},{64,0},{128,64},{192,128},{1,193},{65,1},{129,65},{193,129... | collective-permute-start | bytes 196616 | tf_op jit(solution)/shard_map/ppermute | solution.py:164
  109.7 0.0 collective-permute-done.7
  109.7 1.8 %collective-permute-done.8 = bf16[64,512]{1,0:T(8,128)(2,1)S(1)} collective-permute-done((bf16[64,512]{1,0:T(8,128)(2,1)S(1)}, bf16[64,512]{1,0:T(8,128)(2,1)S(1)}, u32[]{:S(2)}, u32[]{:S(2)}) %collective-permute-start.8) | collective-permute-done | bytes 65568 | tf_op jit(solution)/shard_map/ppermute | solution.py:164
  111.6 3.0 %collective-permute-done.9 = bf16[64,512]{1,0:T(8,128)(2,1)S(1)} collective-permute-done((bf16[64,512]{1,0:T(8,128)(2,1)S(1)}, bf16[64,512]{1,0:T(8,128)(2,1)S(1)}, u32[]{:S(2)}, u32[]{:S(2)}) %collective-permute-start.9) | collective-permute-done | bytes 65568 | tf_op jit(solution)/shard_map/ppermute | solution.py:164
  114.6 0.7 add_convert_fusion
Async XLA Ops:
  0.0 4.7 %collective-permute-start = (bf16[64,512]{1,0:T(8,128)(2,1)}, bf16[64,512]{1,0:T(8,128)(2,1)S(1)}, u32[]{:S(2)}, u32[]{:S(2)}) collective-permute-start(bf16[64,512]{1,0:T(8,128)(2,1)} %own_ref.1), channel_id=1, source_target_pairs={{0,1},{1,0},{2,3},{3,2},{4,5},{5,4},{6,7},{7,6},{8,9},{9,8},{10,11... | collective-permute-start | bytes 196616 | tf_op jit(solution)/shard_map/ppermute | solution.py:161
  4.7 0.9 copy-start.4
  5.7 7.6 %collective-permute-start.3 = (bf16[72,512]{1,0:T(8,128)(2,1)S(1)}, bf16[72,512]{1,0:T(8,128)(2,1)S(1)}, u32[]{:S(2)}, u32[]{:S(2)}) collective-permute-start(bf16[72,512]{1,0:T(8,128)(2,1)S(1)} %shard_map.74.own_ref), channel_id=1, source_target_pairs={{0,192},{64,0},{128,64},{192,128},{1,193},{65,1},{129,65},{193,129... | collective-permute-start | bytes 221192 | tf_op jit(solution)/shard_map/ppermute | solution.py:164
  10.1 7.5 %collective-permute-start.2 = (bf16[72,512]{1,0:T(8,128)(2,1)S(1)}, bf16[72,512]{1,0:T(8,128)(2,1)S(1)}, u32[]{:S(2)}, u32[]{:S(2)}) collective-permute-start(bf16[72,512]{1,0:T(8,128)(2,1)S(1)} %shard_map.74.own_ref), channel_id=1, source_target_pairs={{0,128},{64,192},{128,0},{192,64},{1,129},{65,193},{129,1},{193,65... | collective-permute-start | bytes 221192 | tf_op jit(solution)/shard_map/ppermute | solution.py:164
  11.1 7.4 %collective-permute-start.1 = (bf16[72,512]{1,0:T(8,128)(2,1)S(1)}, bf16[72,512]{1,0:T(8,128)(2,1)S(1)}, u32[]{:S(2)}, u32[]{:S(2)}) collective-permute-start(bf16[72,512]{1,0:T(8,128)(2,1)S(1)} %shard_map.74.own_ref), channel_id=1, source_target_pairs={{0,64},{64,128},{128,192},{192,0},{1,65},{65,129},{129,193},{193,1... | collective-permute-start | bytes 221192 | tf_op jit(solution)/shard_map/ppermute | solution.py:164
  19.5 1.3 %copy-start = (bf16[32,64,512]{2,1,0:T(8,128)(2,1)}, bf16[32,64,512]{2,1,0:T(8,128)(2,1)S(1)}, u32[]{:S(2)}) copy-start(bf16[32,64,512]{2,1,0:T(8,128)(2,1)S(1)} %get-tuple-element.12) | copy-start | bytes 6291460
  20.9 10.6 %copy-start.1 = (bf16[2,1024,256]{2,1,0:T(8,128)(2,1)S(1)}, bf16[2,1024,256]{2,1,0:T(8,128)(2,1)}, u32[]{:S(2)}) copy-start(bf16[2,1024,256]{2,1,0:T(8,128)(2,1)} %gate_ref.1) | copy-start | bytes 3145732
  20.9 38.1 %all-to-all-start = ((bf16[64,32,512]{2,1,0:T(8,128)(2,1)}), bf16[64,32,512]{2,1,0:T(8,128)(2,1)S(1)}, u32[]{:S(2)}, u32[]{:S(2)}) async-start(bf16[64,32,512]{2,1,0:T(8,128)(2,1)} %bitcast.13), calls=%async_computation | async-start | bytes 4194304 | tf_op jit(solution)/shard_map/all_to_all | solution.py:167
  31.5 30.0 %collective-permute-start.4 = (bf16[2,1024,256]{2,1,0:T(8,128)(2,1)S(1)}, bf16[2,1024,256]{2,1,0:T(8,128)(2,1)}, u32[]{:S(2)}, u32[]{:S(2)}) collective-permute-start(bf16[2,1024,256]{2,1,0:T(8,128)(2,1)S(1)} %copy-done.1), channel_id=1, source_target_pairs={{0,1},{1,0},{2,3},{3,2},{4,5},{5,4},{6,7},{7,6},{8,9},{9,8},{10,11... | collective-permute-start | bytes 3145736 | tf_op jit(solution)/shard_map/ppermute | solution.py:161
  32.0 29.5 %collective-permute-start.5 = (bf16[2,1024,256]{2,1,0:T(8,128)(2,1)}, bf16[2,1024,256]{2,1,0:T(8,128)(2,1)}, u32[]{:S(2)}, u32[]{:S(2)}) collective-permute-start(bf16[2,1024,256]{2,1,0:T(8,128)(2,1)} %up_ref.1), channel_id=1, source_target_pairs={{0,1},{1,0},{2,3},{3,2},{4,5},{5,4},{6,7},{7,6},{8,9},{9,8},{10,11... | collective-permute-start | bytes 3145736 | tf_op jit(solution)/shard_map/ppermute | solution.py:161
  32.1 29.4 %collective-permute-start.6 = (bf16[2,512,512]{2,1,0:T(8,128)(2,1)}, bf16[2,512,512]{2,1,0:T(8,128)(2,1)}, u32[]{:S(2)}, u32[]{:S(2)}) collective-permute-start(bf16[2,512,512]{2,1,0:T(8,128)(2,1)} %down_ref.1), channel_id=1, source_target_pairs={{0,1},{1,0},{2,3},{3,2},{4,5},{5,4},{6,7},{7,6},{8,9},{9,8},{10,11... | collective-permute-start | bytes 3145736 | tf_op jit(solution)/shard_map/ppermute | solution.py:161
  59.0 1.2 %copy-start.2 = (bf16[2,1024,256]{2,1,0:T(8,128)(2,1)S(1)}, bf16[2,1024,256]{2,1,0:T(8,128)(2,1)}, u32[]{:S(2)}) copy-start(bf16[2,1024,256]{2,1,0:T(8,128)(2,1)} %up_ref.1) | copy-start | bytes 3145732
  60.2 1.3 %copy-start.3 = (bf16[2,512,512]{2,1,0:T(8,128)(2,1)S(1)}, bf16[2,512,512]{2,1,0:T(8,128)(2,1)}, u32[]{:S(2)}) copy-start(bf16[2,512,512]{2,1,0:T(8,128)(2,1)} %down_ref.1) | copy-start | bytes 3145732
  102.0 7.7 %collective-permute-start.7 = (bf16[64,512]{1,0:T(8,128)(2,1)S(1)}, bf16[64,512]{1,0:T(8,128)(2,1)S(1)}, u32[]{:S(2)}, u32[]{:S(2)}) collective-permute-start(bf16[64,512]{1,0:T(8,128)(2,1)S(1)} %get-tuple-element.16), channel_id=1, source_target_pairs={{0,128},{64,192},{128,0},{192,64},{1,129},{65,193},{129,1},{193,65... | collective-permute-start | bytes 196616 | tf_op jit(solution)/shard_map/ppermute | solution.py:164
  106.2 5.4 %collective-permute-start.8 = (bf16[64,512]{1,0:T(8,128)(2,1)S(1)}, bf16[64,512]{1,0:T(8,128)(2,1)S(1)}, u32[]{:S(2)}, u32[]{:S(2)}) collective-permute-start(bf16[64,512]{1,0:T(8,128)(2,1)S(1)} %get-tuple-element.17), channel_id=1, source_target_pairs={{0,64},{64,128},{128,192},{192,0},{1,65},{65,129},{129,193},{193,1... | collective-permute-start | bytes 196616 | tf_op jit(solution)/shard_map/ppermute | solution.py:164
  107.0 7.7 %collective-permute-start.9 = (bf16[64,512]{1,0:T(8,128)(2,1)S(1)}, bf16[64,512]{1,0:T(8,128)(2,1)S(1)}, u32[]{:S(2)}, u32[]{:S(2)}) collective-permute-start(bf16[64,512]{1,0:T(8,128)(2,1)S(1)} %get-tuple-element.18), channel_id=1, source_target_pairs={{0,192},{64,0},{128,64},{192,128},{1,193},{65,1},{129,65},{193,129... | collective-permute-start | bytes 196616 | tf_op jit(solution)/shard_map/ppermute | solution.py:164
where the time goes:
time: 116 us; the launch traced here: 115 us
  waiting for transfers between devices  36.5 us (31%)
  blocking collectives  34.8 us (30%)
  starting transfers between devices  30.2 us (26%)
  Pallas kernels  9.52 us (8%)
  local copies, waits for them, and re-layouts  3.46 us (3%)
    all_to_all x1, blocking collectives, exchange(): return lax.all_to_all(v, axes, split_axis=0, concat_axis=0, tiled=True)  34.8 us
    all_to_all x1, waiting for transfers between devices, exchange(): return lax.all_to_all(v, axes, split_axis=0, concat_axis=0, tiled=True)  26.5 us
    ppermute x6, starting transfers between devices, shift(): lax.ppermute(v, 'zh', [(i, (i + by) % columns) for i in range(columns)])  15.4 us
    all_to_all x1, starting transfers between devices, exchange(): return lax.all_to_all(v, axes, split_axis=0, concat_axis=0, tiled=True)  10.6 us
    ppermute x6, waiting for transfers between devices, shift(): lax.ppermute(v, 'zh', [(i, (i + by) % columns) for i in range(columns)])  10 us
    pallas_call x7, Pallas kernels, call(): pl.pallas_call(kernel, out_shape=out_shape, cost_estimate=pl.CostEstimate...  9.52 us
    ppermute x4, starting transfers between devices, swap(): return lax.ppermute(v, 'tp', [(0, 1), (1, 0)])  4.25 us
    unnamed x10, local copies, waits for them, and re-layouts  3.46 us
  transfers between devices with their start and end apart: 11, of which 5 were waited for; matrix products, arithmetic and copies ran while one was open for 0% of the time, Pallas kernels for 2%

commit v1 on v0

--- a/solution.py
+++ b/solution.py
@@ -89,17 +89,20 @@
     table_ref[...] = jnp.concatenate(columns + columns, axis=0).T
 
 
+STEP = 512
+
+
 def hidden_part(rows_ref, at, gate_ref, up_ref, core):
     _, _, block, half = rows_ref.shape
-    low, high = (rows_ref[at : at + 256 // block, side].reshape(256, half) for side in range(2))
+    low, high = (rows_ref[at : at + STEP // block, side].reshape(STEP, half) for side in range(2))
     gate, up = (dot(low, ref[core, 0:half, :]) + dot(high, ref[core, half:, :]) for ref in (gate_ref, up_ref))
     return (gate / (1.0 + jnp.exp(-gate)) * up).astype(BF16)
 
 
 def own_kernel(place_ref, rows_ref, gate_ref, up_ref, out_ref):
     chips, _, block, _ = rows_ref.shape
-    for at in range(0, chips, 256 // block):
-        out_ref[at * block : at * block + 256] = hidden_part(rows_ref, at, gate_ref, up_ref, place_ref[0] % 2)
+    for at in range(0, chips, STEP // block):
+        out_ref[at * block : at * block + STEP] = hidden_part(rows_ref, at, gate_ref, up_ref, place_ref[0] % 2)
 
 
 def expert_kernel(place_ref, rows_ref, own_ref, gate2_ref, up2_ref, down_ref, down2_ref, out_ref):
@@ -108,9 +111,9 @@
     width = own_ref.shape[1]
     sides = (core, 1 - core)
     spans = [pl.ds(pl.multiple_of(side * width, width), width) for side in sides]
-    step = 256 // block
+    step = STEP // block
     for at in range(0, chips, step):
-        own = own_ref[at * block : at * block + 256]
+        own = own_ref[at * block : at * block + STEP]
         other = hidden_part(rows_ref, at, gate2_ref, up2_ref, core)
         for side, down in zip(sides, (down_ref, down2_ref)):
             result = dot(own, down[core, spans[0], :]) + dot(other, down[core, spans[1], :])

time: 116 us -> 115 us (level)
  no operation moved by 1% of the time
where the time goes in v1:
time: 115 us
  waiting for transfers between devices  36.5 us (32%)
  blocking collectives  34.8 us (30%)
  starting transfers between devices  30.2 us (26%)
  Pallas kernels  9.11 us (8%)
  local copies, waits for them, and re-layouts  3.46 us (3%)
    all_to_all x1, blocking collectives, exchange(): return lax.all_to_all(v, axes, split_axis=0, concat_axis=0, tiled=True)  34.8 us
    all_to_all x1, waiting for transfers between devices, exchange(): return lax.all_to_all(v, axes, split_axis=0, concat_axis=0, tiled=True)  26.5 us
    ppermute x6, starting transfers between devices, shift(): lax.ppermute(v, 'zh', [(i, (i + by) % columns) for i in range(columns)])  15.4 us
    all_to_all x1, starting transfers between devices, exchange(): return lax.all_to_all(v, axes, split_axis=0, concat_axis=0, tiled=True)  10.6 us
    ppermute x6, waiting for transfers between devices, shift(): lax.ppermute(v, 'zh', [(i, (i + by) % columns) for i in range(columns)])  10 us
    pallas_call x7, Pallas kernels, call(): pl.pallas_call(kernel, out_shape=out_shape, cost_estimate=pl.CostEstimate...  9.11 us
    ppermute x4, starting transfers between devices, swap(): return lax.ppermute(v, 'tp', [(0, 1), (1, 0)])  4.25 us
    unnamed x10, local copies, waits for them, and re-layouts  3.46 us
  transfers between devices with their start and end apart: 11, of which 5 were waited for; matrix products, arithmetic and copies ran while one was open for 0% of the time, Pallas kernels for 2%

profile of v1, /device:TPU:1, one launch (start us, length us, event | category | flops | bytes accessed | tf_op | source)
XLA Modules:
  0.0 114.9 jit_solution(4634818567914634013)
XLA Ops:
  0.0 3.2 %collective-permute-start = (bf16[64,512]{1,0:T(8,128)(2,1)}, bf16[64,512]{1,0:T(8,128)(2,1)S(1)}, u32[]{:S(2)}, u32[]{:S(2)}) collective-permute-start(bf16[64,512]{1,0:T(8,128)(2,1)} %own_ref.1), channel_id=1, source_target_pairs={{0,1},{1,0},{2,3},{3,2},{4,5},{5,4},{6,7},{7,6},{8,9},{9,8},{10,11... | collective-permute-start | bytes 196616 | tf_op jit(solution)/shard_map/ppermute | solution.py:164
  3.2 1.5 %shard_map.73.held_ref = bf16[80,512]{1,0:T(8,128)(2,1)} custom-call(bf16[64,512]{1,0:T(8,128)(2,1)} %own_ref.1, f32[1,512]{1,0:T(1,128)} %bitcast.14, s32[2,64]{1,0:T(2,128)} %bitcast.15, f32[2,64]{1,0:T(2,128)} %bitcast.16), custom_call_target="tpu_custom_call" | custom-call | flops 32768 | bytes 68608 | tf_op jit(solution)/shard_map/pallas_call | solution.py:144
  4.7 0.0 collective-permute-done.other_ref
  4.7 0.0 copy-start.4
  4.7 0.9 copy-done.4
  5.6 0.1 shard_map.74.own_ref
  5.7 4.4 %collective-permute-start.3 = (bf16[72,512]{1,0:T(8,128)(2,1)S(1)}, bf16[72,512]{1,0:T(8,128)(2,1)S(1)}, u32[]{:S(2)}, u32[]{:S(2)}) collective-permute-start(bf16[72,512]{1,0:T(8,128)(2,1)S(1)} %shard_map.74.own_ref), channel_id=1, source_target_pairs={{0,192},{64,0},{128,64},{192,128},{1,193},{65,1},{129,65},{193,129... | collective-permute-start | bytes 221192 | tf_op jit(solution)/shard_map/ppermute | solution.py:167
  10.1 1.0 collective-permute-start.2
  11.1 2.3 %collective-permute-start.1 = (bf16[72,512]{1,0:T(8,128)(2,1)S(1)}, bf16[72,512]{1,0:T(8,128)(2,1)S(1)}, u32[]{:S(2)}, u32[]{:S(2)}) collective-permute-start(bf16[72,512]{1,0:T(8,128)(2,1)S(1)} %shard_map.74.own_ref), channel_id=1, source_target_pairs={{0,64},{64,128},{128,192},{192,0},{1,65},{65,129},{129,193},{193,1... | collective-permute-start | bytes 221192 | tf_op jit(solution)/shard_map/ppermute | solution.py:167
  13.4 0.0 collective-permute-done.3.after_ref
  13.4 4.2 %collective-permute-done.2.opposite_ref = bf16[72,512]{1,0:T(8,128)(2,1)S(1)} collective-permute-done((bf16[72,512]{1,0:T(8,128)(2,1)S(1)}, bf16[72,512]{1,0:T(8,128)(2,1)S(1)}, u32[]{:S(2)}, u32[]{:S(2)}) %collective-permute-start.2) | collective-permute-done | bytes 73760 | tf_op jit(solution)/shard_map/ppermute | solution.py:167
  17.6 0.9 collective-permute-done.1.before_ref
  18.5 1.0 shard_map.75
  19.5 0.0 copy-start
  19.5 1.3 %copy-done = bf16[32,64,512]{2,1,0:T(8,128)(2,1)} copy-done((bf16[32,64,512]{2,1,0:T(8,128)(2,1)}, bf16[32,64,512]{2,1,0:T(8,128)(2,1)S(1)}, u32[]{:S(2)}) %copy-start) | copy-done | bytes 2097176
  20.9 0.0 copy-start.1
  20.9 10.6 %all-to-all-start = ((bf16[64,32,512]{2,1,0:T(8,128)(2,1)}), bf16[64,32,512]{2,1,0:T(8,128)(2,1)S(1)}, u32[]{:S(2)}, u32[]{:S(2)}) async-start(bf16[64,32,512]{2,1,0:T(8,128)(2,1)} %bitcast.13), calls=%async_computation | async-start | bytes 4194304 | tf_op jit(solution)/shard_map/all_to_all | solution.py:170
  31.5 0.0 copy-done.1
  31.5 0.5 collective-permute-start.4
  32.0 0.1 collective-permute-start.5
  32.1 0.4 collective-permute-start.6
  32.5 26.5 %all-to-all-done = bf16[64,32,512]{2,1,0:T(8,128)(2,1)S(1)} async-done(((bf16[64,32,512]{2,1,0:T(8,128)(2,1)}), bf16[64,32,512]{2,1,0:T(8,128)(2,1)S(1)}, u32[]{:S(2)}, u32[]{:S(2)}) %all-to-all-start) | async-done | bytes 2097184 | tf_op jit(solution)/shard_map/all_to_all | solution.py:170
  59.0 0.0 copy-start.2
  59.0 1.2 %copy-done.2 = bf16[2,1024,256]{2,1,0:T(8,128)(2,1)S(1)} copy-done((bf16[2,1024,256]{2,1,0:T(8,128)(2,1)S(1)}, bf16[2,1024,256]{2,1,0:T(8,128)(2,1)}, u32[]{:S(2)}) %copy-start.2) | copy-done | bytes 1048600
  60.2 0.0 copy-start.3
  60.2 1.3 %shard_map.76.own_ref = bf16[1024,256]{1,0:T(8,128)(2,1)S(1)} custom-call(s32[1]{0:T(128)} %bitcast.place_ref, bf16[32,2,32,512]{3,2,1,0:T(8,128)(2,1)S(1)} %bitcast.8, bf16[2,1024,256]{2,1,0:T(8,128)(2,1)S(1)} %copy-done.1, bf16[2,1024,256]{2,1,0:T(8,128)(2,1)S(1)} %copy-done.2), custom_call_target="tpu_custom_call" | custom-call | flops 1073741824 | bytes 4194308 | tf_op jit(solution)/shard_map/pallas_call | solution.py:144
  61.5 0.0 collective-permute-done.4.gate2_ref
  61.5 0.0 collective-permute-done.5.up2_ref
  61.5 0.0 collective-permute-done.6.down2_ref
  61.5 0.0 copy-done.3
  61.5 4.2 %shard_map.77 = bf16[32,2,32,512]{3,2,1,0:T(8,128)(2,1)S(1)} custom-call(s32[1]{0:T(128)} %bitcast.place_ref, bf16[32,2,32,512]{3,2,1,0:T(8,128)(2,1)S(1)} %bitcast.9, bf16[1024,256]{1,0:T(8,128)(2,1)S(1)} %shard_map.76.own_ref, bf16[2,1024,256]{2,1,0:T(8,128)(2,1)} %collective-permute-done.4.gate2_ref, ...), custom_call_target="tpu_custom_call" | custom-call | flops 2147483648 | bytes 6815748 | tf_op jit(solution)/shard_map/pallas_call | solution.py:144
  65.8 34.8 %all_to_all.10 = bf16[64,32,512]{2,1,0:T(8,128)(2,1)S(1)} all-to-all(bf16[64,32,512]{2,1,0:T(8,128)(2,1)S(1)} %bitcast.12), channel_id=1, replica_groups=mesh['zh'=4,'zl'=2,'y'=4,'x'=4,'tp'=2] {'zl','y','x','tp'}, dimensions={0} | all-to-all | bytes 4194304 | tf_op jit(solution)/shard_map/all_to_all | solution.py:170
  100.6 0.5 shard_map.79
  101.1 0.5 shard_map.78
  101.6 4.2 %collective-permute-start.7 = (bf16[64,512]{1,0:T(8,128)(2,1)S(1)}, bf16[64,512]{1,0:T(8,128)(2,1)S(1)}, u32[]{:S(2)}, u32[]{:S(2)}) collective-permute-start(bf16[64,512]{1,0:T(8,128)(2,1)S(1)} %get-tuple-element.16), channel_id=1, source_target_pairs={{0,128},{64,192},{128,0},{192,64},{1,129},{65,193},{129,1},{193,65... | collective-permute-start | bytes 196616 | tf_op jit(solution)/shard_map/ppermute | solution.py:167
  105.7 0.8 collective-permute-start.8
  106.5 2.8 %collective-permute-start.9 = (bf16[64,512]{1,0:T(8,128)(2,1)S(1)}, bf16[64,512]{1,0:T(8,128)(2,1)S(1)}, u32[]{:S(2)}, u32[]{:S(2)}) collective-permute-start(bf16[64,512]{1,0:T(8,128)(2,1)S(1)} %get-tuple-element.18), channel_id=1, source_target_pairs={{0,192},{64,0},{128,64},{192,128},{1,193},{65,1},{129,65},{193,129... | collective-permute-start | bytes 196616 | tf_op jit(solution)/shard_map/ppermute | solution.py:167
  109.3 0.0 collective-permute-done.7
  109.3 1.8 %collective-permute-done.8 = bf16[64,512]{1,0:T(8,128)(2,1)S(1)} collective-permute-done((bf16[64,512]{1,0:T(8,128)(2,1)S(1)}, bf16[64,512]{1,0:T(8,128)(2,1)S(1)}, u32[]{:S(2)}, u32[]{:S(2)}) %collective-permute-start.8) | collective-permute-done | bytes 65568 | tf_op jit(solution)/shard_map/ppermute | solution.py:167
  111.2 3.0 %collective-permute-done.9 = bf16[64,512]{1,0:T(8,128)(2,1)S(1)} collective-permute-done((bf16[64,512]{1,0:T(8,128)(2,1)S(1)}, bf16[64,512]{1,0:T(8,128)(2,1)S(1)}, u32[]{:S(2)}, u32[]{:S(2)}) %collective-permute-start.9) | collective-permute-done | bytes 65568 | tf_op jit(solution)/shard_map/ppermute | solution.py:167
  114.2 0.7 add_convert_fusion
Async XLA Ops:
  0.0 4.7 %collective-permute-start = (bf16[64,512]{1,0:T(8,128)(2,1)}, bf16[64,512]{1,0:T(8,128)(2,1)S(1)}, u32[]{:S(2)}, u32[]{:S(2)}) collective-permute-start(bf16[64,512]{1,0:T(8,128)(2,1)} %own_ref.1), channel_id=1, source_target_pairs={{0,1},{1,0},{2,3},{3,2},{4,5},{5,4},{6,7},{7,6},{8,9},{9,8},{10,11... | collective-permute-start | bytes 196616 | tf_op jit(solution)/shard_map/ppermute | solution.py:164
  4.7 0.9 copy-start.4
  5.7 7.6 %collective-permute-start.3 = (bf16[72,512]{1,0:T(8,128)(2,1)S(1)}, bf16[72,512]{1,0:T(8,128)(2,1)S(1)}, u32[]{:S(2)}, u32[]{:S(2)}) collective-permute-start(bf16[72,512]{1,0:T(8,128)(2,1)S(1)} %shard_map.74.own_ref), channel_id=1, source_target_pairs={{0,192},{64,0},{128,64},{192,128},{1,193},{65,1},{129,65},{193,129... | collective-permute-start | bytes 221192 | tf_op jit(solution)/shard_map/ppermute | solution.py:167
  10.1 7.5 %collective-permute-start.2 = (bf16[72,512]{1,0:T(8,128)(2,1)S(1)}, bf16[72,512]{1,0:T(8,128)(2,1)S(1)}, u32[]{:S(2)}, u32[]{:S(2)}) collective-permute-start(bf16[72,512]{1,0:T(8,128)(2,1)S(1)} %shard_map.74.own_ref), channel_id=1, source_target_pairs={{0,128},{64,192},{128,0},{192,64},{1,129},{65,193},{129,1},{193,65... | collective-permute-start | bytes 221192 | tf_op jit(solution)/shard_map/ppermute | solution.py:167
  11.1 7.4 %collective-permute-start.1 = (bf16[72,512]{1,0:T(8,128)(2,1)S(1)}, bf16[72,512]{1,0:T(8,128)(2,1)S(1)}, u32[]{:S(2)}, u32[]{:S(2)}) collective-permute-start(bf16[72,512]{1,0:T(8,128)(2,1)S(1)} %shard_map.74.own_ref), channel_id=1, source_target_pairs={{0,64},{64,128},{128,192},{192,0},{1,65},{65,129},{129,193},{193,1... | collective-permute-start | bytes 221192 | tf_op jit(solution)/shard_map/ppermute | solution.py:167
  19.5 1.3 %copy-start = (bf16[32,64,512]{2,1,0:T(8,128)(2,1)}, bf16[32,64,512]{2,1,0:T(8,128)(2,1)S(1)}, u32[]{:S(2)}) copy-start(bf16[32,64,512]{2,1,0:T(8,128)(2,1)S(1)} %get-tuple-element.12) | copy-start | bytes 6291460
  20.9 10.6 %copy-start.1 = (bf16[2,1024,256]{2,1,0:T(8,128)(2,1)S(1)}, bf16[2,1024,256]{2,1,0:T(8,128)(2,1)}, u32[]{:S(2)}) copy-start(bf16[2,1024,256]{2,1,0:T(8,128)(2,1)} %gate_ref.1) | copy-start | bytes 3145732
  20.9 38.1 %all-to-all-start = ((bf16[64,32,512]{2,1,0:T(8,128)(2,1)}), bf16[64,32,512]{2,1,0:T(8,128)(2,1)S(1)}, u32[]{:S(2)}, u32[]{:S(2)}) async-start(bf16[64,32,512]{2,1,0:T(8,128)(2,1)} %bitcast.13), calls=%async_computation | async-start | bytes 4194304 | tf_op jit(solution)/shard_map/all_to_all | solution.py:170
  31.5 30.0 %collective-permute-start.4 = (bf16[2,1024,256]{2,1,0:T(8,128)(2,1)S(1)}, bf16[2,1024,256]{2,1,0:T(8,128)(2,1)}, u32[]{:S(2)}, u32[]{:S(2)}) collective-permute-start(bf16[2,1024,256]{2,1,0:T(8,128)(2,1)S(1)} %copy-done.1), channel_id=1, source_target_pairs={{0,1},{1,0},{2,3},{3,2},{4,5},{5,4},{6,7},{7,6},{8,9},{9,8},{10,11... | collective-permute-start | bytes 3145736 | tf_op jit(solution)/shard_map/ppermute | solution.py:164
  32.0 29.5 %collective-permute-start.5 = (bf16[2,1024,256]{2,1,0:T(8,128)(2,1)}, bf16[2,1024,256]{2,1,0:T(8,128)(2,1)}, u32[]{:S(2)}, u32[]{:S(2)}) collective-permute-start(bf16[2,1024,256]{2,1,0:T(8,128)(2,1)} %up_ref.1), channel_id=1, source_target_pairs={{0,1},{1,0},{2,3},{3,2},{4,5},{5,4},{6,7},{7,6},{8,9},{9,8},{10,11... | collective-permute-start | bytes 3145736 | tf_op jit(solution)/shard_map/ppermute | solution.py:164
  32.1 29.4 %collective-permute-start.6 = (bf16[2,512,512]{2,1,0:T(8,128)(2,1)}, bf16[2,512,512]{2,1,0:T(8,128)(2,1)}, u32[]{:S(2)}, u32[]{:S(2)}) collective-permute-start(bf16[2,512,512]{2,1,0:T(8,128)(2,1)} %down_ref.1), channel_id=1, source_target_pairs={{0,1},{1,0},{2,3},{3,2},{4,5},{5,4},{6,7},{7,6},{8,9},{9,8},{10,11... | collective-permute-start | bytes 3145736 | tf_op jit(solution)/shard_map/ppermute | solution.py:164
  59.0 1.2 %copy-start.2 = (bf16[2,1024,256]{2,1,0:T(8,128)(2,1)S(1)}, bf16[2,1024,256]{2,1,0:T(8,128)(2,1)}, u32[]{:S(2)}) copy-start(bf16[2,1024,256]{2,1,0:T(8,128)(2,1)} %up_ref.1) | copy-start | bytes 3145732
  60.2 1.3 %copy-start.3 = (bf16[2,512,512]{2,1,0:T(8,128)(2,1)S(1)}, bf16[2,512,512]{2,1,0:T(8,128)(2,1)}, u32[]{:S(2)}) copy-start(bf16[2,512,512]{2,1,0:T(8,128)(2,1)} %down_ref.1) | copy-start | bytes 3145732
  101.6 7.7 %collective-permute-start.7 = (bf16[64,512]{1,0:T(8,128)(2,1)S(1)}, bf16[64,512]{1,0:T(8,128)(2,1)S(1)}, u32[]{:S(2)}, u32[]{:S(2)}) collective-permute-start(bf16[64,512]{1,0:T(8,128)(2,1)S(1)} %get-tuple-element.16), channel_id=1, source_target_pairs={{0,128},{64,192},{128,0},{192,64},{1,129},{65,193},{129,1},{193,65... | collective-permute-start | bytes 196616 | tf_op jit(solution)/shard_map/ppermute | solution.py:167
  105.7 5.4 %collective-permute-start.8 = (bf16[64,512]{1,0:T(8,128)(2,1)S(1)}, bf16[64,512]{1,0:T(8,128)(2,1)S(1)}, u32[]{:S(2)}, u32[]{:S(2)}) collective-permute-start(bf16[64,512]{1,0:T(8,128)(2,1)S(1)} %get-tuple-element.17), channel_id=1, source_target_pairs={{0,64},{64,128},{128,192},{192,0},{1,65},{65,129},{129,193},{193,1... | collective-permute-start | bytes 196616 | tf_op jit(solution)/shard_map/ppermute | solution.py:167
  106.5 7.7 %collective-permute-start.9 = (bf16[64,512]{1,0:T(8,128)(2,1)S(1)}, bf16[64,512]{1,0:T(8,128)(2,1)S(1)}, u32[]{:S(2)}, u32[]{:S(2)}) collective-permute-start(bf16[64,512]{1,0:T(8,128)(2,1)S(1)} %get-tuple-element.18), channel_id=1, source_target_pairs={{0,192},{64,0},{128,64},{192,128},{1,193},{65,1},{129,65},{193,129... | collective-permute-start | bytes 196616 | tf_op jit(solution)/shard_map/ppermute | solution.py:167

commit v2 on v1

--- a/solution.py
+++ b/solution.py
@@ -54,9 +54,9 @@
     out_ref[rows:, :] = tail[0:INFO, :]
 
 
-def dispatch_kernel(place_ref, own_ref, before_ref, opposite_ref, after_ref, out_ref, table0_ref, table1_ref):
-    place_pair(0, place_ref, own_ref, before_ref, out_ref, table0_ref)
-    place_pair(1, place_ref, opposite_ref, after_ref, out_ref, table1_ref)
+def dispatch_kernel(place_ref, own_ref, first_ref, third_ref, second_ref, out_ref, table0_ref, table1_ref):
+    place_pair(0, place_ref, own_ref, first_ref, out_ref, table0_ref)
+    place_pair(1, place_ref, third_ref, second_ref, out_ref, table1_ref)
 
 
 def place_pair(pair, place_ref, a_ref, b_ref, out_ref, table_ref):
@@ -163,8 +163,10 @@
     def swap(v):
         return lax.ppermute(v, "tp", [(0, 1), (1, 0)])
 
-    def shift(v, by):
-        return lax.ppermute(v, "zh", [(i, (i + by) % columns) for i in range(columns)])
+    def relay(v, by, home=False):
+        planes = lax.axis_size(("zh", "zl"))
+        pairs = [(z, (z - by if z % 2 else z + by) % planes) for z in range(planes)]
+        return lax.ppermute(v, ("zh", "zl"), [(to, z) for z, to in pairs] if home else pairs)
 
     def exchange(v, axes):
         return lax.all_to_all(v, axes, split_axis=0, concat_axis=0, tiled=True)
@@ -179,14 +181,14 @@
         60,
     )
     own = call(norm_kernel, jax.ShapeDtypeStruct((rows + INFO, half), BF16), (held, other), rows * half, 4)
-    opposite = shift(own, 2)
-    before, after = shift(own, 1), shift(own, -1)
+    third = relay(own, -3)
+    second, first = relay(own, 2), relay(own, -1)
 
     buffer = jax.ShapeDtypeStruct((peers, block, half), BF16)
     small = jax.ShapeDtypeStruct((2 * rows, 8), F32)
     flops = total * 2 * rows * half
     sent, table0, table1 = call(
-        dispatch_kernel, (buffer, small, small), (place, own, before, opposite, after), 2 * flops, 12, 1
+        dispatch_kernel, (buffer, small, small), (place, own, first, third, second), 2 * flops, 12, 1
     )
     arrived = exchange(sent.reshape(2 * peers, block // 2, half), plane)
     arrived = arrived.reshape(peers, 2, block // 2, half)
@@ -209,10 +211,10 @@
     back = exchange(result.reshape(2 * peers, block // 2, half), plane)
     back = back.reshape(peers, block, half)
     pair = (jax.ShapeDtypeStruct((rows, half), BF16),) * 2
-    opposite, after = call(functools.partial(combine_kernel, 1), pair, (back, table1), 2 * flops, 8)
-    own, before = call(functools.partial(combine_kernel, 0), pair, (back, table0), 2 * flops, 8)
-    home = [shift(opposite, -2)]
-    home += [shift(after, 1), shift(before, -1)]
+    third, second = call(functools.partial(combine_kernel, 1), pair, (back, table1), 2 * flops, 8)
+    home = [relay(third, -3, home=True)]
+    own, first = call(functools.partial(combine_kernel, 0), pair, (back, table0), 2 * flops, 8)
+    home += [relay(second, 2, home=True), relay(first, -1, home=True)]
     return sum((part.astype(F32) for part in home), own.astype(F32)).astype(BF16)
 
 

time: 115 us -> 111 us (0.965)
  the two profiles are of different devices: /device:TPU:1 before, /device:TPU:32 now
where the time goes in v2:
time: 111 us; the launch traced here: 110 us
  waiting for transfers between devices  37.7 us (34%)
  blocking collectives  34.8 us (31%)
  starting transfers between devices  23.9 us (22%)
  Pallas kernels  9.13 us (8%)
  local copies, waits for them, and re-layouts  3.45 us (3%)
    all_to_all x1, blocking collectives, exchange(): return lax.all_to_all(v, axes, split_axis=0, concat_axis=0, tiled=True)  34.8 us
    all_to_all x1, waiting for transfers between devices, exchange(): return lax.all_to_all(v, axes, split_axis=0, concat_axis=0, tiled=True)  26.5 us
    ppermute x6, starting transfers between devices, relay(): lax.ppermute(v, ('zh', 'zl'), [(to, z) for z, to in pairs] if home else p...  14 us
    ppermute x6, waiting for transfers between devices, relay(): lax.ppermute(v, ('zh', 'zl'), [(to, z) for z, to in pairs] if home else p...  11.1 us
    all_to_all x1, starting transfers between devices, exchange(): return lax.all_to_all(v, axes, split_axis=0, concat_axis=0, tiled=True)  9.19 us
    pallas_call x7, Pallas kernels, call(): pl.pallas_call(kernel, out_shape=out_shape, cost_estimate=pl.CostEstimate...  9.13 us
    unnamed x10, local copies, waits for them, and re-layouts  3.45 us
  transfers between devices with their start and end apart: 11, of which 5 were waited for; matrix products, arithmetic and copies ran while one was open for 0% of the time, Pallas kernels for 3%

profile of v2, /device:TPU:32, one launch (start us, length us, event | category | flops | bytes accessed | tf_op | source)
XLA Modules:
  0.0 109.8 jit_solution(2434285389788003337)
XLA Ops:
  0.0 0.0 collective-permute-start
  0.0 1.5 %shard_map.73.held_ref = bf16[80,512]{1,0:T(8,128)(2,1)} custom-call(bf16[64,512]{1,0:T(8,128)(2,1)} %own_ref.1, f32[1,512]{1,0:T(1,128)} %bitcast.14, s32[2,64]{1,0:T(2,128)} %bitcast.15, f32[2,64]{1,0:T(2,128)} %bitcast.16), custom_call_target="tpu_custom_call" | custom-call | flops 32768 | bytes 68608 | tf_op jit(solution)/shard_map/pallas_call | solution.py:144
  1.5 0.0 collective-permute-done.other_ref
  1.5 0.0 copy-start.4
  1.5 0.9 copy-done.4
  2.4 0.1 shard_map.74.own_ref
  2.5 5.5 %collective-permute-start.3 = (bf16[72,512]{1,0:T(8,128)(2,1)S(1)}, bf16[72,512]{1,0:T(8,128)(2,1)S(1)}, u32[]{:S(2)}, u32[]{:S(2)}) collective-permute-start(bf16[72,512]{1,0:T(8,128)(2,1)S(1)} %shard_map.74.own_ref), channel_id=1, source_target_pairs={{0,64},{32,224},{64,128},{96,32},{128,192},{160,96},{192,0},{224,1... | collective-permute-start | bytes 221192 | tf_op jit(solution)/shard_map/ppermute | solution.py:169
  8.0 1.9 %collective-permute-start.2 = (bf16[72,512]{1,0:T(8,128)(2,1)S(1)}, bf16[72,512]{1,0:T(8,128)(2,1)S(1)}, u32[]{:S(2)}, u32[]{:S(2)}) collective-permute-start(bf16[72,512]{1,0:T(8,128)(2,1)S(1)} %shard_map.74.own_ref), channel_id=1, source_target_pairs={{0,160},{32,128},{64,224},{96,192},{128,32},{160,0},{192,96},{224,... | collective-permute-start | bytes 221192 | tf_op jit(solution)/shard_map/ppermute | solution.py:169
  9.9 1.0 collective-permute-start.1
  10.9 0.0 collective-permute-done.3.second_ref
  10.9 5.5 %collective-permute-done.2.third_ref = bf16[72,512]{1,0:T(8,128)(2,1)S(1)} collective-permute-done((bf16[72,512]{1,0:T(8,128)(2,1)S(1)}, bf16[72,512]{1,0:T(8,128)(2,1)S(1)}, u32[]{:S(2)}, u32[]{:S(2)}) %collective-permute-start.2) | collective-permute-done | bytes 73760 | tf_op jit(solution)/shard_map/ppermute | solution.py:169
  16.4 0.0 collective-permute-done.1.first_ref
  16.5 1.0 shard_map.75
  17.5 0.0 copy-start
  17.5 1.3 %copy-done = bf16[32,64,512]{2,1,0:T(8,128)(2,1)} copy-done((bf16[32,64,512]{2,1,0:T(8,128)(2,1)}, bf16[32,64,512]{2,1,0:T(8,128)(2,1)S(1)}, u32[]{:S(2)}) %copy-start) | copy-done | bytes 2097176
  18.9 0.0 copy-start.1
  18.9 9.2 %all-to-all-start = ((bf16[64,32,512]{2,1,0:T(8,128)(2,1)}), bf16[64,32,512]{2,1,0:T(8,128)(2,1)S(1)}, u32[]{:S(2)}, u32[]{:S(2)}) async-start(bf16[64,32,512]{2,1,0:T(8,128)(2,1)} %bitcast.13), calls=%async_computation | async-start | bytes 4194304 | tf_op jit(solution)/shard_map/all_to_all | solution.py:172
  28.1 0.0 copy-done.1
  28.1 0.2 collective-permute-start.4
  28.3 0.4 collective-permute-start.5
  28.7 0.1 collective-permute-start.6
  28.8 26.5 %all-to-all-done = bf16[64,32,512]{2,1,0:T(8,128)(2,1)S(1)} async-done(((bf16[64,32,512]{2,1,0:T(8,128)(2,1)}), bf16[64,32,512]{2,1,0:T(8,128)(2,1)S(1)}, u32[]{:S(2)}, u32[]{:S(2)}) %all-to-all-start) | async-done | bytes 2097184 | tf_op jit(solution)/shard_map/all_to_all | solution.py:172
  55.3 0.0 copy-start.2
  55.3 1.2 %copy-done.2 = bf16[2,1024,256]{2,1,0:T(8,128)(2,1)S(1)} copy-done((bf16[2,1024,256]{2,1,0:T(8,128)(2,1)S(1)}, bf16[2,1024,256]{2,1,0:T(8,128)(2,1)}, u32[]{:S(2)}) %copy-start.2) | copy-done | bytes 1048600
  56.5 0.0 copy-start.3
  56.6 1.3 %shard_map.76.own_ref = bf16[1024,256]{1,0:T(8,128)(2,1)S(1)} custom-call(s32[1]{0:T(128)} %bitcast.place_ref, bf16[32,2,32,512]{3,2,1,0:T(8,128)(2,1)S(1)} %bitcast.8, bf16[2,1024,256]{2,1,0:T(8,128)(2,1)S(1)} %copy-done.1, bf16[2,1024,256]{2,1,0:T(8,128)(2,1)S(1)} %copy-done.2), custom_call_target="tpu_custom_call" | custom-call | flops 1073741824 | bytes 4194308 | tf_op jit(solution)/shard_map/pallas_call | solution.py:144
  57.8 0.0 collective-permute-done.4.gate2_ref
  57.8 0.0 collective-permute-done.5.up2_ref
  57.8 0.0 collective-permute-done.6.down2_ref
  57.9 0.0 copy-done.3
  57.9 4.2 %shard_map.77 = bf16[32,2,32,512]{3,2,1,0:T(8,128)(2,1)S(1)} custom-call(s32[1]{0:T(128)} %bitcast.place_ref, bf16[32,2,32,512]{3,2,1,0:T(8,128)(2,1)S(1)} %bitcast.9, bf16[1024,256]{1,0:T(8,128)(2,1)S(1)} %shard_map.76.own_ref, bf16[2,1024,256]{2,1,0:T(8,128)(2,1)} %collective-permute-done.4.gate2_ref, ...), custom_call_target="tpu_custom_call" | custom-call | flops 2147483648 | bytes 6815748 | tf_op jit(solution)/shard_map/pallas_call | solution.py:144
  62.1 34.8 %all_to_all.10 = bf16[64,32,512]{2,1,0:T(8,128)(2,1)S(1)} all-to-all(bf16[64,32,512]{2,1,0:T(8,128)(2,1)S(1)} %bitcast.12), channel_id=1, replica_groups=mesh['zh'=4,'zl'=2,'y'=4,'x'=4,'tp'=2] {'zl','y','x','tp'}, dimensions={0} | all-to-all | bytes 4194304 | tf_op jit(solution)/shard_map/all_to_all | solution.py:172
  96.9 0.5 shard_map.79
  97.4 0.5 shard_map.78
  97.9 2.9 %collective-permute-start.7 = (bf16[64,512]{1,0:T(8,128)(2,1)S(1)}, bf16[64,512]{1,0:T(8,128)(2,1)S(1)}, u32[]{:S(2)}, u32[]{:S(2)}) collective-permute-start(bf16[64,512]{1,0:T(8,128)(2,1)S(1)} %get-tuple-element.16), channel_id=1, source_target_pairs={{160,0},{128,32},{224,64},{192,96},{32,128},{0,160},{96,192},{64,2... | collective-permute-start | bytes 196616 | tf_op jit(solution)/shard_map/ppermute | solution.py:169
  100.8 1.9 %collective-permute-start.8 = (bf16[64,512]{1,0:T(8,128)(2,1)S(1)}, bf16[64,512]{1,0:T(8,128)(2,1)S(1)}, u32[]{:S(2)}, u32[]{:S(2)}) collective-permute-start(bf16[64,512]{1,0:T(8,128)(2,1)S(1)} %get-tuple-element.17), channel_id=1, source_target_pairs={{64,0},{224,32},{128,64},{32,96},{192,128},{96,160},{0,192},{160,2... | collective-permute-start | bytes 196616 | tf_op jit(solution)/shard_map/ppermute | solution.py:169
  102.7 0.8 collective-permute-start.9
  103.5 3.0 %collective-permute-done.7 = bf16[64,512]{1,0:T(8,128)(2,1)S(1)} collective-permute-done((bf16[64,512]{1,0:T(8,128)(2,1)S(1)}, bf16[64,512]{1,0:T(8,128)(2,1)S(1)}, u32[]{:S(2)}, u32[]{:S(2)}) %collective-permute-start.7) | collective-permute-done | bytes 65568 | tf_op jit(solution)/shard_map/ppermute | solution.py:169
  106.5 1.1 %collective-permute-done.8 = bf16[64,512]{1,0:T(8,128)(2,1)S(1)} collective-permute-done((bf16[64,512]{1,0:T(8,128)(2,1)S(1)}, bf16[64,512]{1,0:T(8,128)(2,1)S(1)}, u32[]{:S(2)}, u32[]{:S(2)}) %collective-permute-start.8) | collective-permute-done | bytes 65568 | tf_op jit(solution)/shard_map/ppermute | solution.py:169
  107.6 1.5 %collective-permute-done.9 = bf16[64,512]{1,0:T(8,128)(2,1)S(1)} collective-permute-done((bf16[64,512]{1,0:T(8,128)(2,1)S(1)}, bf16[64,512]{1,0:T(8,128)(2,1)S(1)}, u32[]{:S(2)}, u32[]{:S(2)}) %collective-permute-start.9) | collective-permute-done | bytes 65568 | tf_op jit(solution)/shard_map/ppermute | solution.py:169
  109.1 0.7 add_convert_fusion
Async XLA Ops:
  0.0 1.5 %collective-permute-start = (bf16[64,512]{1,0:T(8,128)(2,1)}, bf16[64,512]{1,0:T(8,128)(2,1)S(1)}, u32[]{:S(2)}, u32[]{:S(2)}) collective-permute-start(bf16[64,512]{1,0:T(8,128)(2,1)} %own_ref.1), channel_id=1, source_target_pairs={{0,1},{1,0},{2,3},{3,2},{4,5},{5,4},{6,7},{7,6},{8,9},{9,8},{10,11... | collective-permute-start | bytes 196616 | tf_op jit(solution)/shard_map/ppermute | solution.py:164
  1.5 0.9 copy-start.4
  2.5 8.4 %collective-permute-start.3 = (bf16[72,512]{1,0:T(8,128)(2,1)S(1)}, bf16[72,512]{1,0:T(8,128)(2,1)S(1)}, u32[]{:S(2)}, u32[]{:S(2)}) collective-permute-start(bf16[72,512]{1,0:T(8,128)(2,1)S(1)} %shard_map.74.own_ref), channel_id=1, source_target_pairs={{0,64},{32,224},{64,128},{96,32},{128,192},{160,96},{192,0},{224,1... | collective-permute-start | bytes 221192 | tf_op jit(solution)/shard_map/ppermute | solution.py:169
  8.0 8.4 %collective-permute-start.2 = (bf16[72,512]{1,0:T(8,128)(2,1)S(1)}, bf16[72,512]{1,0:T(8,128)(2,1)S(1)}, u32[]{:S(2)}, u32[]{:S(2)}) collective-permute-start(bf16[72,512]{1,0:T(8,128)(2,1)S(1)} %shard_map.74.own_ref), channel_id=1, source_target_pairs={{0,160},{32,128},{64,224},{96,192},{128,32},{160,0},{192,96},{224,... | collective-permute-start | bytes 221192 | tf_op jit(solution)/shard_map/ppermute | solution.py:169
  9.9 6.5 %collective-permute-start.1 = (bf16[72,512]{1,0:T(8,128)(2,1)S(1)}, bf16[72,512]{1,0:T(8,128)(2,1)S(1)}, u32[]{:S(2)}, u32[]{:S(2)}) collective-permute-start(bf16[72,512]{1,0:T(8,128)(2,1)S(1)} %shard_map.74.own_ref), channel_id=1, source_target_pairs={{0,224},{32,64},{64,32},{96,128},{128,96},{160,192},{192,160},{224... | collective-permute-start | bytes 221192 | tf_op jit(solution)/shard_map/ppermute | solution.py:169
  17.5 1.3 %copy-start = (bf16[32,64,512]{2,1,0:T(8,128)(2,1)}, bf16[32,64,512]{2,1,0:T(8,128)(2,1)S(1)}, u32[]{:S(2)}) copy-start(bf16[32,64,512]{2,1,0:T(8,128)(2,1)S(1)} %get-tuple-element.12) | copy-start | bytes 6291460
  18.9 9.2 %copy-start.1 = (bf16[2,1024,256]{2,1,0:T(8,128)(2,1)S(1)}, bf16[2,1024,256]{2,1,0:T(8,128)(2,1)}, u32[]{:S(2)}) copy-start(bf16[2,1024,256]{2,1,0:T(8,128)(2,1)} %gate_ref.1) | copy-start | bytes 3145732
  18.9 36.5 %all-to-all-start = ((bf16[64,32,512]{2,1,0:T(8,128)(2,1)}), bf16[64,32,512]{2,1,0:T(8,128)(2,1)S(1)}, u32[]{:S(2)}, u32[]{:S(2)}) async-start(bf16[64,32,512]{2,1,0:T(8,128)(2,1)} %bitcast.13), calls=%async_computation | async-start | bytes 4194304 | tf_op jit(solution)/shard_map/all_to_all | solution.py:172
  28.1 29.8 %collective-permute-start.4 = (bf16[2,1024,256]{2,1,0:T(8,128)(2,1)S(1)}, bf16[2,1024,256]{2,1,0:T(8,128)(2,1)}, u32[]{:S(2)}, u32[]{:S(2)}) collective-permute-start(bf16[2,1024,256]{2,1,0:T(8,128)(2,1)S(1)} %copy-done.1), channel_id=1, source_target_pairs={{0,1},{1,0},{2,3},{3,2},{4,5},{5,4},{6,7},{7,6},{8,9},{9,8},{10,11... | collective-permute-start | bytes 3145736 | tf_op jit(solution)/shard_map/ppermute | solution.py:164
  28.3 29.6 %collective-permute-start.5 = (bf16[2,1024,256]{2,1,0:T(8,128)(2,1)}, bf16[2,1024,256]{2,1,0:T(8,128)(2,1)}, u32[]{:S(2)}, u32[]{:S(2)}) collective-permute-start(bf16[2,1024,256]{2,1,0:T(8,128)(2,1)} %up_ref.1), channel_id=1, source_target_pairs={{0,1},{1,0},{2,3},{3,2},{4,5},{5,4},{6,7},{7,6},{8,9},{9,8},{10,11... | collective-permute-start | bytes 3145736 | tf_op jit(solution)/shard_map/ppermute | solution.py:164
  28.7 29.2 %collective-permute-start.6 = (bf16[2,512,512]{2,1,0:T(8,128)(2,1)}, bf16[2,512,512]{2,1,0:T(8,128)(2,1)}, u32[]{:S(2)}, u32[]{:S(2)}) collective-permute-start(bf16[2,512,512]{2,1,0:T(8,128)(2,1)} %down_ref.1), channel_id=1, source_target_pairs={{0,1},{1,0},{2,3},{3,2},{4,5},{5,4},{6,7},{7,6},{8,9},{9,8},{10,11... | collective-permute-start | bytes 3145736 | tf_op jit(solution)/shard_map/ppermute | solution.py:164
  55.3 1.2 %copy-start.2 = (bf16[2,1024,256]{2,1,0:T(8,128)(2,1)S(1)}, bf16[2,1024,256]{2,1,0:T(8,128)(2,1)}, u32[]{:S(2)}) copy-start(bf16[2,1024,256]{2,1,0:T(8,128)(2,1)} %up_ref.1) | copy-start | bytes 3145732
  56.5 1.3 %copy-start.3 = (bf16[2,512,512]{2,1,0:T(8,128)(2,1)S(1)}, bf16[2,512,512]{2,1,0:T(8,128)(2,1)}, u32[]{:S(2)}) copy-start(bf16[2,512,512]{2,1,0:T(8,128)(2,1)} %down_ref.1) | copy-start | bytes 3145732
  97.9 8.6 %collective-permute-start.7 = (bf16[64,512]{1,0:T(8,128)(2,1)S(1)}, bf16[64,512]{1,0:T(8,128)(2,1)S(1)}, u32[]{:S(2)}, u32[]{:S(2)}) collective-permute-start(bf16[64,512]{1,0:T(8,128)(2,1)S(1)} %get-tuple-element.16), channel_id=1, source_target_pairs={{160,0},{128,32},{224,64},{192,96},{32,128},{0,160},{96,192},{64,2... | collective-permute-start | bytes 196616 | tf_op jit(solution)/shard_map/ppermute | solution.py:169
  100.8 6.9 %collective-permute-start.8 = (bf16[64,512]{1,0:T(8,128)(2,1)S(1)}, bf16[64,512]{1,0:T(8,128)(2,1)S(1)}, u32[]{:S(2)}, u32[]{:S(2)}) collective-permute-start(bf16[64,512]{1,0:T(8,128)(2,1)S(1)} %get-tuple-element.17), channel_id=1, source_target_pairs={{64,0},{224,32},{128,64},{32,96},{192,128},{96,160},{0,192},{160,2... | collective-permute-start | bytes 196616 | tf_op jit(solution)/shard_map/ppermute | solution.py:169
  102.7 6.4 %collective-permute-start.9 = (bf16[64,512]{1,0:T(8,128)(2,1)S(1)}, bf16[64,512]{1,0:T(8,128)(2,1)S(1)}, u32[]{:S(2)}, u32[]{:S(2)}) collective-permute-start(bf16[64,512]{1,0:T(8,128)(2,1)S(1)} %get-tuple-element.18), channel_id=1, source_target_pairs={{224,0},{64,32},{32,64},{128,96},{96,128},{192,160},{160,192},{0,2... | collective-permute-start | bytes 196616 | tf_op jit(solution)/shard_map/ppermute | solution.py:169

commit v3 on v2

--- a/solution.py
+++ b/solution.py
@@ -123,15 +123,16 @@
 def combine_kernel(pair, back_ref, table_ref, a_ref, b_ref):
     rows, half = a_ref.shape
     peers, block, _ = back_ref.shape
-    picked = [None, None]
+    picked = None
     for local in range(2):
         at = local * (block // 2) + 16 * pair
         back = back_ref[:, at : at + 16, :].reshape(16 * peers, half)
         place = iota((2 * rows, 16 * peers), 1) + local * 16 * peers
-        for k in range(2):
-            term = dot(one_hot(place == table_ref[:, k : k + 1].astype(jnp.int32)), back)
-            picked[k] = term if picked[k] is None else picked[k] + term
-    total = (picked[0] * table_ref[:, 2:3] + picked[1] * table_ref[:, 3:4]).astype(BF16)
+        chosen = [one_hot(place == table_ref[:, k : k + 1].astype(jnp.int32)) for k in range(2)]
+        term = dot(jnp.concatenate(chosen, axis=0), back)
+        picked = term if picked is None else picked + term
+    total = picked[0 : 2 * rows] * table_ref[:, 2:3] + picked[2 * rows :] * table_ref[:, 3:4]
+    total = total.astype(BF16)
     a_ref[...] = total[0:rows]
     b_ref[...] = total[rows:]
 
@@ -182,7 +183,8 @@
     )
     own = call(norm_kernel, jax.ShapeDtypeStruct((rows + INFO, half), BF16), (held, other), rows * half, 4)
     third = relay(own, -3)
-    second, first = relay(own, 2), relay(own, -1)
+    first = relay(own, -1)
+    second = relay(own, 2)
 
     buffer = jax.ShapeDtypeStruct((peers, block, half), BF16)
     small = jax.ShapeDtypeStruct((2 * rows, 8), F32)
@@ -213,8 +215,9 @@
     pair = (jax.ShapeDtypeStruct((rows, half), BF16),) * 2
     third, second = call(functools.partial(combine_kernel, 1), pair, (back, table1), 2 * flops, 8)
     home = [relay(third, -3, home=True)]
+    home += [relay(second, 2, home=True)]
     own, first = call(functools.partial(combine_kernel, 0), pair, (back, table0), 2 * flops, 8)
-    home += [relay(second, 2, home=True), relay(first, -1, home=True)]
+    home += [relay(first, -1, home=True)]
     return sum((part.astype(F32) for part in home), own.astype(F32)).astype(BF16)
 
 

time: 111 us -> 111 us (level)
  no operation moved by 1% of the time
where the time goes in v3:
time: 111 us; the launch traced here: 110 us
  waiting for transfers between devices  37.7 us (34%)
  blocking collectives  34.8 us (31%)
  starting transfers between devices  23.9 us (22%)
  Pallas kernels  9.17 us (8%)
  local copies, waits for them, and re-layouts  3.45 us (3%)
    all_to_all x1, blocking collectives, exchange(): return lax.all_to_all(v, axes, split_axis=0, concat_axis=0, tiled=True)  34.8 us
    all_to_all x1, waiting for transfers between devices, exchange(): return lax.all_to_all(v, axes, split_axis=0, concat_axis=0, tiled=True)  26.5 us
    ppermute x6, starting transfers between devices, relay(): lax.ppermute(v, ('zh', 'zl'), [(to, z) for z, to in pairs] if home else p...  14 us
    ppermute x6, waiting for transfers between devices, relay(): lax.ppermute(v, ('zh', 'zl'), [(to, z) for z, to in pairs] if home else p...  11.1 us
    all_to_all x1, starting transfers between devices, exchange(): return lax.all_to_all(v, axes, split_axis=0, concat_axis=0, tiled=True)  9.19 us
    pallas_call x7, Pallas kernels, call(): pl.pallas_call(kernel, out_shape=out_shape, cost_estimate=pl.CostEstimate...  9.17 us
    unnamed x10, local copies, waits for them, and re-layouts  3.45 us
  transfers between devices with their start and end apart: 11, of which 5 were waited for; matrix products, arithmetic and copies ran while one was open for 0% of the time, Pallas kernels for 3%

profile of v3, /device:TPU:32, one launch (start us, length us, event | category | flops | bytes accessed | tf_op | source)
XLA Modules:
  0.0 109.8 jit_solution(5895276745955658875)
XLA Ops:
  0.0 0.0 collective-permute-start
  0.0 1.5 %shard_map.73.held_ref = bf16[80,512]{1,0:T(8,128)(2,1)} custom-call(bf16[64,512]{1,0:T(8,128)(2,1)} %own_ref.1, f32[1,512]{1,0:T(1,128)} %bitcast.14, s32[2,64]{1,0:T(2,128)} %bitcast.15, f32[2,64]{1,0:T(2,128)} %bitcast.16), custom_call_target="tpu_custom_call" | custom-call | flops 32768 | bytes 68608 | tf_op jit(solution)/shard_map/pallas_call | solution.py:145
  1.5 0.0 collective-permute-done.other_ref
  1.5 0.0 copy-start.4
  1.5 0.9 copy-done.4
  2.4 0.1 shard_map.74.own_ref
  2.5 5.5 %collective-permute-start.3 = (bf16[72,512]{1,0:T(8,128)(2,1)S(1)}, bf16[72,512]{1,0:T(8,128)(2,1)S(1)}, u32[]{:S(2)}, u32[]{:S(2)}) collective-permute-start(bf16[72,512]{1,0:T(8,128)(2,1)S(1)} %shard_map.74.own_ref), channel_id=1, source_target_pairs={{0,64},{32,224},{64,128},{96,32},{128,192},{160,96},{192,0},{224,1... | collective-permute-start | bytes 221192 | tf_op jit(solution)/shard_map/ppermute | solution.py:170
  8.0 1.9 %collective-permute-start.2 = (bf16[72,512]{1,0:T(8,128)(2,1)S(1)}, bf16[72,512]{1,0:T(8,128)(2,1)S(1)}, u32[]{:S(2)}, u32[]{:S(2)}) collective-permute-start(bf16[72,512]{1,0:T(8,128)(2,1)S(1)} %shard_map.74.own_ref), channel_id=1, source_target_pairs={{0,160},{32,128},{64,224},{96,192},{128,32},{160,0},{192,96},{224,... | collective-permute-start | bytes 221192 | tf_op jit(solution)/shard_map/ppermute | solution.py:170
  9.9 1.0 collective-permute-start.1
  10.9 0.0 collective-permute-done.3.second_ref
  10.9 5.5 %collective-permute-done.2.third_ref = bf16[72,512]{1,0:T(8,128)(2,1)S(1)} collective-permute-done((bf16[72,512]{1,0:T(8,128)(2,1)S(1)}, bf16[72,512]{1,0:T(8,128)(2,1)S(1)}, u32[]{:S(2)}, u32[]{:S(2)}) %collective-permute-start.2) | collective-permute-done | bytes 73760 | tf_op jit(solution)/shard_map/ppermute | solution.py:170
  16.4 0.0 collective-permute-done.1.first_ref
  16.5 1.0 shard_map.75
  17.5 0.0 copy-start
  17.5 1.3 %copy-done = bf16[32,64,512]{2,1,0:T(8,128)(2,1)} copy-done((bf16[32,64,512]{2,1,0:T(8,128)(2,1)}, bf16[32,64,512]{2,1,0:T(8,128)(2,1)S(1)}, u32[]{:S(2)}) %copy-start) | copy-done | bytes 2097176
  18.9 0.0 copy-start.1
  18.9 9.2 %all-to-all-start = ((bf16[64,32,512]{2,1,0:T(8,128)(2,1)}), bf16[64,32,512]{2,1,0:T(8,128)(2,1)S(1)}, u32[]{:S(2)}, u32[]{:S(2)}) async-start(bf16[64,32,512]{2,1,0:T(8,128)(2,1)} %bitcast.13), calls=%async_computation | async-start | bytes 4194304 | tf_op jit(solution)/shard_map/all_to_all | solution.py:173
  28.1 0.0 copy-done.1
  28.1 0.2 collective-permute-start.4
  28.3 0.4 collective-permute-start.5
  28.7 0.1 collective-permute-start.6
  28.8 26.5 %all-to-all-done = bf16[64,32,512]{2,1,0:T(8,128)(2,1)S(1)} async-done(((bf16[64,32,512]{2,1,0:T(8,128)(2,1)}), bf16[64,32,512]{2,1,0:T(8,128)(2,1)S(1)}, u32[]{:S(2)}, u32[]{:S(2)}) %all-to-all-start) | async-done | bytes 2097184 | tf_op jit(solution)/shard_map/all_to_all | solution.py:173
  55.3 0.0 copy-start.2
  55.3 1.2 %copy-done.2 = bf16[2,1024,256]{2,1,0:T(8,128)(2,1)S(1)} copy-done((bf16[2,1024,256]{2,1,0:T(8,128)(2,1)S(1)}, bf16[2,1024,256]{2,1,0:T(8,128)(2,1)}, u32[]{:S(2)}) %copy-start.2) | copy-done | bytes 1048600
  56.5 0.0 copy-start.3
  56.6 1.3 %shard_map.76.own_ref = bf16[1024,256]{1,0:T(8,128)(2,1)S(1)} custom-call(s32[1]{0:T(128)} %bitcast.place_ref, bf16[32,2,32,512]{3,2,1,0:T(8,128)(2,1)S(1)} %bitcast.8, bf16[2,1024,256]{2,1,0:T(8,128)(2,1)S(1)} %copy-done.1, bf16[2,1024,256]{2,1,0:T(8,128)(2,1)S(1)} %copy-done.2), custom_call_target="tpu_custom_call" | custom-call | flops 1073741824 | bytes 4194308 | tf_op jit(solution)/shard_map/pallas_call | solution.py:145
  57.8 0.0 collective-permute-done.4.gate2_ref
  57.8 0.0 collective-permute-done.5.up2_ref
  57.8 0.0 collective-permute-done.6.down2_ref
  57.9 0.0 copy-done.3
  57.9 4.2 %shard_map.77 = bf16[32,2,32,512]{3,2,1,0:T(8,128)(2,1)S(1)} custom-call(s32[1]{0:T(128)} %bitcast.place_ref, bf16[32,2,32,512]{3,2,1,0:T(8,128)(2,1)S(1)} %bitcast.9, bf16[1024,256]{1,0:T(8,128)(2,1)S(1)} %shard_map.76.own_ref, bf16[2,1024,256]{2,1,0:T(8,128)(2,1)} %collective-permute-done.4.gate2_ref, ...), custom_call_target="tpu_custom_call" | custom-call | flops 2147483648 | bytes 6815748 | tf_op jit(solution)/shard_map/pallas_call | solution.py:145
  62.1 34.8 %all_to_all.10 = bf16[64,32,512]{2,1,0:T(8,128)(2,1)S(1)} all-to-all(bf16[64,32,512]{2,1,0:T(8,128)(2,1)S(1)} %bitcast.12), channel_id=1, replica_groups=mesh['zh'=4,'zl'=2,'y'=4,'x'=4,'tp'=2] {'zl','y','x','tp'}, dimensions={0} | all-to-all | bytes 4194304 | tf_op jit(solution)/shard_map/all_to_all | solution.py:173
  96.9 0.5 shard_map.79
  97.4 0.5 shard_map.78
  97.9 2.9 %collective-permute-start.7 = (bf16[64,512]{1,0:T(8,128)(2,1)S(1)}, bf16[64,512]{1,0:T(8,128)(2,1)S(1)}, u32[]{:S(2)}, u32[]{:S(2)}) collective-permute-start(bf16[64,512]{1,0:T(8,128)(2,1)S(1)} %get-tuple-element.16), channel_id=1, source_target_pairs={{160,0},{128,32},{224,64},{192,96},{32,128},{0,160},{96,192},{64,2... | collective-permute-start | bytes 196616 | tf_op jit(solution)/shard_map/ppermute | solution.py:170
  100.8 1.9 %collective-permute-start.8 = (bf16[64,512]{1,0:T(8,128)(2,1)S(1)}, bf16[64,512]{1,0:T(8,128)(2,1)S(1)}, u32[]{:S(2)}, u32[]{:S(2)}) collective-permute-start(bf16[64,512]{1,0:T(8,128)(2,1)S(1)} %get-tuple-element.17), channel_id=1, source_target_pairs={{64,0},{224,32},{128,64},{32,96},{192,128},{96,160},{0,192},{160,2... | collective-permute-start | bytes 196616 | tf_op jit(solution)/shard_map/ppermute | solution.py:170
  102.7 0.8 collective-permute-start.9
  103.6 3.0 %collective-permute-done.7 = bf16[64,512]{1,0:T(8,128)(2,1)S(1)} collective-permute-done((bf16[64,512]{1,0:T(8,128)(2,1)S(1)}, bf16[64,512]{1,0:T(8,128)(2,1)S(1)}, u32[]{:S(2)}, u32[]{:S(2)}) %collective-permute-start.7) | collective-permute-done | bytes 65568 | tf_op jit(solution)/shard_map/ppermute | solution.py:170
  106.6 1.1 %collective-permute-done.8 = bf16[64,512]{1,0:T(8,128)(2,1)S(1)} collective-permute-done((bf16[64,512]{1,0:T(8,128)(2,1)S(1)}, bf16[64,512]{1,0:T(8,128)(2,1)S(1)}, u32[]{:S(2)}, u32[]{:S(2)}) %collective-permute-start.8) | collective-permute-done | bytes 65568 | tf_op jit(solution)/shard_map/ppermute | solution.py:170
  107.7 1.5 %collective-permute-done.9 = bf16[64,512]{1,0:T(8,128)(2,1)S(1)} collective-permute-done((bf16[64,512]{1,0:T(8,128)(2,1)S(1)}, bf16[64,512]{1,0:T(8,128)(2,1)S(1)}, u32[]{:S(2)}, u32[]{:S(2)}) %collective-permute-start.9) | collective-permute-done | bytes 65568 | tf_op jit(solution)/shard_map/ppermute | solution.py:170
  109.2 0.7 add_convert_fusion
Async XLA Ops:
  0.0 1.5 %collective-permute-start = (bf16[64,512]{1,0:T(8,128)(2,1)}, bf16[64,512]{1,0:T(8,128)(2,1)S(1)}, u32[]{:S(2)}, u32[]{:S(2)}) collective-permute-start(bf16[64,512]{1,0:T(8,128)(2,1)} %own_ref.1), channel_id=1, source_target_pairs={{0,1},{1,0},{2,3},{3,2},{4,5},{5,4},{6,7},{7,6},{8,9},{9,8},{10,11... | collective-permute-start | bytes 196616 | tf_op jit(solution)/shard_map/ppermute | solution.py:165
  1.5 0.9 copy-start.4
  2.5 8.4 %collective-permute-start.3 = (bf16[72,512]{1,0:T(8,128)(2,1)S(1)}, bf16[72,512]{1,0:T(8,128)(2,1)S(1)}, u32[]{:S(2)}, u32[]{:S(2)}) collective-permute-start(bf16[72,512]{1,0:T(8,128)(2,1)S(1)} %shard_map.74.own_ref), channel_id=1, source_target_pairs={{0,64},{32,224},{64,128},{96,32},{128,192},{160,96},{192,0},{224,1... | collective-permute-start | bytes 221192 | tf_op jit(solution)/shard_map/ppermute | solution.py:170
  8.0 8.4 %collective-permute-start.2 = (bf16[72,512]{1,0:T(8,128)(2,1)S(1)}, bf16[72,512]{1,0:T(8,128)(2,1)S(1)}, u32[]{:S(2)}, u32[]{:S(2)}) collective-permute-start(bf16[72,512]{1,0:T(8,128)(2,1)S(1)} %shard_map.74.own_ref), channel_id=1, source_target_pairs={{0,160},{32,128},{64,224},{96,192},{128,32},{160,0},{192,96},{224,... | collective-permute-start | bytes 221192 | tf_op jit(solution)/shard_map/ppermute | solution.py:170
  9.9 6.5 %collective-permute-start.1 = (bf16[72,512]{1,0:T(8,128)(2,1)S(1)}, bf16[72,512]{1,0:T(8,128)(2,1)S(1)}, u32[]{:S(2)}, u32[]{:S(2)}) collective-permute-start(bf16[72,512]{1,0:T(8,128)(2,1)S(1)} %shard_map.74.own_ref), channel_id=1, source_target_pairs={{0,224},{32,64},{64,32},{96,128},{128,96},{160,192},{192,160},{224... | collective-permute-start | bytes 221192 | tf_op jit(solution)/shard_map/ppermute | solution.py:170
  17.5 1.3 %copy-start = (bf16[32,64,512]{2,1,0:T(8,128)(2,1)}, bf16[32,64,512]{2,1,0:T(8,128)(2,1)S(1)}, u32[]{:S(2)}) copy-start(bf16[32,64,512]{2,1,0:T(8,128)(2,1)S(1)} %get-tuple-element.12) | copy-start | bytes 6291460
  18.9 9.2 %copy-start.1 = (bf16[2,1024,256]{2,1,0:T(8,128)(2,1)S(1)}, bf16[2,1024,256]{2,1,0:T(8,128)(2,1)}, u32[]{:S(2)}) copy-start(bf16[2,1024,256]{2,1,0:T(8,128)(2,1)} %gate_ref.1) | copy-start | bytes 3145732
  18.9 36.5 %all-to-all-start = ((bf16[64,32,512]{2,1,0:T(8,128)(2,1)}), bf16[64,32,512]{2,1,0:T(8,128)(2,1)S(1)}, u32[]{:S(2)}, u32[]{:S(2)}) async-start(bf16[64,32,512]{2,1,0:T(8,128)(2,1)} %bitcast.13), calls=%async_computation | async-start | bytes 4194304 | tf_op jit(solution)/shard_map/all_to_all | solution.py:173
  28.1 29.8 %collective-permute-start.4 = (bf16[2,1024,256]{2,1,0:T(8,128)(2,1)S(1)}, bf16[2,1024,256]{2,1,0:T(8,128)(2,1)}, u32[]{:S(2)}, u32[]{:S(2)}) collective-permute-start(bf16[2,1024,256]{2,1,0:T(8,128)(2,1)S(1)} %copy-done.1), channel_id=1, source_target_pairs={{0,1},{1,0},{2,3},{3,2},{4,5},{5,4},{6,7},{7,6},{8,9},{9,8},{10,11... | collective-permute-start | bytes 3145736 | tf_op jit(solution)/shard_map/ppermute | solution.py:165
  28.3 29.6 %collective-permute-start.5 = (bf16[2,1024,256]{2,1,0:T(8,128)(2,1)}, bf16[2,1024,256]{2,1,0:T(8,128)(2,1)}, u32[]{:S(2)}, u32[]{:S(2)}) collective-permute-start(bf16[2,1024,256]{2,1,0:T(8,128)(2,1)} %up_ref.1), channel_id=1, source_target_pairs={{0,1},{1,0},{2,3},{3,2},{4,5},{5,4},{6,7},{7,6},{8,9},{9,8},{10,11... | collective-permute-start | bytes 3145736 | tf_op jit(solution)/shard_map/ppermute | solution.py:165
  28.7 29.2 %collective-permute-start.6 = (bf16[2,512,512]{2,1,0:T(8,128)(2,1)}, bf16[2,512,512]{2,1,0:T(8,128)(2,1)}, u32[]{:S(2)}, u32[]{:S(2)}) collective-permute-start(bf16[2,512,512]{2,1,0:T(8,128)(2,1)} %down_ref.1), channel_id=1, source_target_pairs={{0,1},{1,0},{2,3},{3,2},{4,5},{5,4},{6,7},{7,6},{8,9},{9,8},{10,11... | collective-permute-start | bytes 3145736 | tf_op jit(solution)/shard_map/ppermute | solution.py:165
  55.3 1.2 %copy-start.2 = (bf16[2,1024,256]{2,1,0:T(8,128)(2,1)S(1)}, bf16[2,1024,256]{2,1,0:T(8,128)(2,1)}, u32[]{:S(2)}) copy-start(bf16[2,1024,256]{2,1,0:T(8,128)(2,1)} %up_ref.1) | copy-start | bytes 3145732
  56.5 1.3 %copy-start.3 = (bf16[2,512,512]{2,1,0:T(8,128)(2,1)S(1)}, bf16[2,512,512]{2,1,0:T(8,128)(2,1)}, u32[]{:S(2)}) copy-start(bf16[2,512,512]{2,1,0:T(8,128)(2,1)} %down_ref.1) | copy-start | bytes 3145732
  97.9 8.6 %collective-permute-start.7 = (bf16[64,512]{1,0:T(8,128)(2,1)S(1)}, bf16[64,512]{1,0:T(8,128)(2,1)S(1)}, u32[]{:S(2)}, u32[]{:S(2)}) collective-permute-start(bf16[64,512]{1,0:T(8,128)(2,1)S(1)} %get-tuple-element.16), channel_id=1, source_target_pairs={{160,0},{128,32},{224,64},{192,96},{32,128},{0,160},{96,192},{64,2... | collective-permute-start | bytes 196616 | tf_op jit(solution)/shard_map/ppermute | solution.py:170
  100.8 6.9 %collective-permute-start.8 = (bf16[64,512]{1,0:T(8,128)(2,1)S(1)}, bf16[64,512]{1,0:T(8,128)(2,1)S(1)}, u32[]{:S(2)}, u32[]{:S(2)}) collective-permute-start(bf16[64,512]{1,0:T(8,128)(2,1)S(1)} %get-tuple-element.17), channel_id=1, source_target_pairs={{64,0},{224,32},{128,64},{32,96},{192,128},{96,160},{0,192},{160,2... | collective-permute-start | bytes 196616 | tf_op jit(solution)/shard_map/ppermute | solution.py:170
  102.7 6.4 %collective-permute-start.9 = (bf16[64,512]{1,0:T(8,128)(2,1)S(1)}, bf16[64,512]{1,0:T(8,128)(2,1)S(1)}, u32[]{:S(2)}, u32[]{:S(2)}) collective-permute-start(bf16[64,512]{1,0:T(8,128)(2,1)S(1)} %get-tuple-element.18), channel_id=1, source_target_pairs={{224,0},{64,32},{32,64},{128,96},{96,128},{192,160},{160,192},{0,2... | collective-permute-start | bytes 196616 | tf_op jit(solution)/shard_map/ppermute | solution.py:170

commit v4 on v3

--- a/solution.py
+++ b/solution.py
@@ -54,12 +54,18 @@
     out_ref[rows:, :] = tail[0:INFO, :]
 
 
-def dispatch_kernel(place_ref, own_ref, first_ref, third_ref, second_ref, out_ref, table0_ref, table1_ref):
-    place_pair(0, place_ref, own_ref, first_ref, out_ref, table0_ref)
-    place_pair(1, place_ref, third_ref, second_ref, out_ref, table1_ref)
-
-
-def place_pair(pair, place_ref, a_ref, b_ref, out_ref, table_ref):
+def early_kernel(place_ref, own_ref, first_ref, rows_ref, table_ref):
+    place_pair(place_ref, own_ref, first_ref, rows_ref, table_ref)
+
+
+def dispatch_kernel(place_ref, third_ref, second_ref, early_ref, out_ref, table_ref):
+    for local in range(2):
+        at = local * out_ref.shape[1] // 2
+        out_ref[:, at : at + 16, :] = early_ref[:, 16 * local : 16 * (local + 1), :]
+    place_pair(place_ref, third_ref, second_ref, out_ref, table_ref, 16)
+
+
+def place_pair(place_ref, a_ref, b_ref, out_ref, table_ref, start=0):
     rows = a_ref.shape[0] - INFO
     span = 2 * rows
     peers, block, half = out_ref.shape
@@ -81,7 +87,7 @@
         slots.append(jnp.where((pick >= 0) & (pick < experts), slot, -1))
         weights.append(info[2 + k : 3 + k] + info[4 + k : 5 + k] + info[6 + k : 7 + k])
     for local in range(2):
-        at = local * (block // 2) + 16 * pair
+        at = local * (block // 2) + start
         slot = iota((16 * peers, span), 0) + local * 16 * peers
         sent = dot(one_hot((slot == slots[0]) | (slot == slots[1])), tokens)
         out_ref[:, at : at + 16, :] = sent.astype(BF16).reshape(peers, 16, half)
@@ -189,9 +195,15 @@
     buffer = jax.ShapeDtypeStruct((peers, block, half), BF16)
     small = jax.ShapeDtypeStruct((2 * rows, 8), F32)
     flops = total * 2 * rows * half
-    sent, table0, table1 = call(
-        dispatch_kernel, (buffer, small, small), (place, own, first, third, second), 2 * flops, 12, 1
-    )
+    early, table0 = call(
+        early_kernel,
+        (jax.ShapeDtypeStruct((peers, block // 2, half), BF16), small),
+        (place, own, first),
+        flops,
+        8,
+        1,
+    )
+    sent, table1 = call(dispatch_kernel, (buffer, small), (place, third, second, early), flops, 8, 1)
     arrived = exchange(sent.reshape(2 * peers, block // 2, half), plane)
     arrived = arrived.reshape(peers, 2, block // 2, half)
     hidden = call(

time: 111 us -> 112 us (level)
    pallas_call x7 -> x8, Pallas kernels: 9.17 us -> 9.48 us  [call(): pl.pallas_call(kernel, out_shape=out_shape, cost_estimate=pl.CostEstimate...]
where the time goes in v4:
time: 112 us; the launch traced here: 110 us
  waiting for transfers between devices  38 us (34%)
  blocking collectives  34.8 us (31%)
  starting transfers between devices  23.3 us (21%)
  Pallas kernels  9.48 us (8%)
  local copies, waits for them, and re-layouts  3.45 us (3%)
    all_to_all x1, blocking collectives, exchange(): return lax.all_to_all(v, axes, split_axis=0, concat_axis=0, tiled=True)  34.8 us
    all_to_all x1, waiting for transfers between devices, exchange(): return lax.all_to_all(v, axes, split_axis=0, concat_axis=0, tiled=True)  26.5 us
    ppermute x6, starting transfers between devices, relay(): lax.ppermute(v, ('zh', 'zl'), [(to, z) for z, to in pairs] if home else p...  13.4 us
    ppermute x6, waiting for transfers between devices, relay(): lax.ppermute(v, ('zh', 'zl'), [(to, z) for z, to in pairs] if home else p...  11.5 us
    pallas_call x8, Pallas kernels, call(): pl.pallas_call(kernel, out_shape=out_shape, cost_estimate=pl.CostEstimate...  9.48 us
    all_to_all x1, starting transfers between devices, exchange(): return lax.all_to_all(v, axes, split_axis=0, concat_axis=0, tiled=True)  9.17 us
    unnamed x10, local copies, waits for them, and re-layouts  3.45 us
  transfers between devices with their start and end apart: 11, of which 5 were waited for; matrix products, arithmetic and copies ran while one was open for 0% of the time, Pallas kernels for 3%

profile of v4, /device:TPU:32, one launch (start us, length us, event | category | flops | bytes accessed | tf_op | source)
XLA Modules:
  0.0 109.9 jit_solution(4602306291854988432)
XLA Ops:
  0.0 0.0 collective-permute-start
  0.0 1.5 %shard_map.73.held_ref = bf16[80,512]{1,0:T(8,128)(2,1)} custom-call(bf16[64,512]{1,0:T(8,128)(2,1)} %own_ref.1, f32[1,512]{1,0:T(1,128)} %bitcast.14, s32[2,64]{1,0:T(2,128)} %bitcast.15, f32[2,64]{1,0:T(2,128)} %bitcast.16), custom_call_target="tpu_custom_call" | custom-call | flops 32768 | bytes 68608 | tf_op jit(solution)/shard_map/pallas_call | solution.py:151
  1.5 0.0 collective-permute-done.other_ref
  1.5 0.0 copy-start.4
  1.5 0.9 copy-done.4
  2.4 0.1 shard_map.74.own_ref
  2.5 2.0 %collective-permute-start.3 = (bf16[72,512]{1,0:T(8,128)(2,1)S(1)}, bf16[72,512]{1,0:T(8,128)(2,1)S(1)}, u32[]{:S(2)}, u32[]{:S(2)}) collective-permute-start(bf16[72,512]{1,0:T(8,128)(2,1)S(1)} %shard_map.74.own_ref), channel_id=1, source_target_pairs={{0,224},{32,64},{64,32},{96,128},{128,96},{160,192},{192,160},{224... | collective-permute-start | bytes 221192 | tf_op jit(solution)/shard_map/ppermute | solution.py:176
  4.5 3.6 %collective-permute-start.2 = (bf16[72,512]{1,0:T(8,128)(2,1)S(1)}, bf16[72,512]{1,0:T(8,128)(2,1)S(1)}, u32[]{:S(2)}, u32[]{:S(2)}) collective-permute-start(bf16[72,512]{1,0:T(8,128)(2,1)S(1)} %shard_map.74.own_ref), channel_id=1, source_target_pairs={{0,64},{32,224},{64,128},{96,32},{128,192},{160,96},{192,0},{224,1... | collective-permute-start | bytes 221192 | tf_op jit(solution)/shard_map/ppermute | solution.py:176
  8.1 2.8 %collective-permute-start.1 = (bf16[72,512]{1,0:T(8,128)(2,1)S(1)}, bf16[72,512]{1,0:T(8,128)(2,1)S(1)}, u32[]{:S(2)}, u32[]{:S(2)}) collective-permute-start(bf16[72,512]{1,0:T(8,128)(2,1)S(1)} %shard_map.74.own_ref), channel_id=1, source_target_pairs={{0,160},{32,128},{64,224},{96,192},{128,32},{160,0},{192,96},{224,... | collective-permute-start | bytes 221192 | tf_op jit(solution)/shard_map/ppermute | solution.py:176
  10.9 0.0 collective-permute-done.3.first_ref
  10.9 0.6 shard_map.75
  11.6 0.1 collective-permute-done.2.second_ref
  11.7 6.4 %collective-permute-done.1.third_ref = bf16[72,512]{1,0:T(8,128)(2,1)S(1)} collective-permute-done((bf16[72,512]{1,0:T(8,128)(2,1)S(1)}, bf16[72,512]{1,0:T(8,128)(2,1)S(1)}, u32[]{:S(2)}, u32[]{:S(2)}) %collective-permute-start.1) | collective-permute-done | bytes 73760 | tf_op jit(solution)/shard_map/ppermute | solution.py:176
  18.1 0.7 shard_map.76
  18.9 0.0 copy-start
  18.9 1.3 %copy-done = bf16[32,64,512]{2,1,0:T(8,128)(2,1)} copy-done((bf16[32,64,512]{2,1,0:T(8,128)(2,1)}, bf16[32,64,512]{2,1,0:T(8,128)(2,1)S(1)}, u32[]{:S(2)}) %copy-start) | copy-done | bytes 2097176
  20.2 0.0 copy-start.1
  20.2 9.2 %all-to-all-start = ((bf16[64,32,512]{2,1,0:T(8,128)(2,1)}), bf16[64,32,512]{2,1,0:T(8,128)(2,1)S(1)}, u32[]{:S(2)}, u32[]{:S(2)}) async-start(bf16[64,32,512]{2,1,0:T(8,128)(2,1)} %bitcast.13), calls=%async_computation | async-start | bytes 4194304 | tf_op jit(solution)/shard_map/all_to_all | solution.py:179
  29.4 0.0 copy-done.1
  29.4 0.2 collective-permute-start.4
  29.6 0.4 collective-permute-start.5
  30.0 0.1 collective-permute-start.6
  30.1 26.5 %all-to-all-done = bf16[64,32,512]{2,1,0:T(8,128)(2,1)S(1)} async-done(((bf16[64,32,512]{2,1,0:T(8,128)(2,1)}), bf16[64,32,512]{2,1,0:T(8,128)(2,1)S(1)}, u32[]{:S(2)}, u32[]{:S(2)}) %all-to-all-start) | async-done | bytes 2097184 | tf_op jit(solution)/shard_map/all_to_all | solution.py:179
  56.7 0.0 copy-start.2
  56.7 1.2 %copy-done.2 = bf16[2,1024,256]{2,1,0:T(8,128)(2,1)S(1)} copy-done((bf16[2,1024,256]{2,1,0:T(8,128)(2,1)S(1)}, bf16[2,1024,256]{2,1,0:T(8,128)(2,1)}, u32[]{:S(2)}) %copy-start.2) | copy-done | bytes 1048600
  57.9 0.0 copy-start.3
  57.9 1.3 %shard_map.77.own_ref = bf16[1024,256]{1,0:T(8,128)(2,1)S(1)} custom-call(s32[1]{0:T(128)} %bitcast.place_ref, bf16[32,2,32,512]{3,2,1,0:T(8,128)(2,1)S(1)} %bitcast.8, bf16[2,1024,256]{2,1,0:T(8,128)(2,1)S(1)} %copy-done.1, bf16[2,1024,256]{2,1,0:T(8,128)(2,1)S(1)} %copy-done.2), custom_call_target="tpu_custom_call" | custom-call | flops 1073741824 | bytes 4194308 | tf_op jit(solution)/shard_map/pallas_call | solution.py:151
  59.2 0.0 collective-permute-done.4.gate2_ref
  59.2 0.0 collective-permute-done.5.up2_ref
  59.2 0.0 collective-permute-done.6.down2_ref
  59.2 0.0 copy-done.3
  59.2 4.2 %shard_map.78 = bf16[32,2,32,512]{3,2,1,0:T(8,128)(2,1)S(1)} custom-call(s32[1]{0:T(128)} %bitcast.place_ref, bf16[32,2,32,512]{3,2,1,0:T(8,128)(2,1)S(1)} %bitcast.9, bf16[1024,256]{1,0:T(8,128)(2,1)S(1)} %shard_map.77.own_ref, bf16[2,1024,256]{2,1,0:T(8,128)(2,1)} %collective-permute-done.4.gate2_ref, ...), custom_call_target="tpu_custom_call" | custom-call | flops 2147483648 | bytes 6815748 | tf_op jit(solution)/shard_map/pallas_call | solution.py:151
  63.4 34.8 %all_to_all.10 = bf16[64,32,512]{2,1,0:T(8,128)(2,1)S(1)} all-to-all(bf16[64,32,512]{2,1,0:T(8,128)(2,1)S(1)} %bitcast.12), channel_id=1, replica_groups=mesh['zh'=4,'zl'=2,'y'=4,'x'=4,'tp'=2] {'zl','y','x','tp'}, dimensions={0} | all-to-all | bytes 4194304 | tf_op jit(solution)/shard_map/all_to_all | solution.py:179
  98.2 0.5 shard_map.80
  98.8 0.5 shard_map.79
  99.3 2.3 %collective-permute-start.7 = (bf16[64,512]{1,0:T(8,128)(2,1)S(1)}, bf16[64,512]{1,0:T(8,128)(2,1)S(1)}, u32[]{:S(2)}, u32[]{:S(2)}) collective-permute-start(bf16[64,512]{1,0:T(8,128)(2,1)S(1)} %get-tuple-element.18), channel_id=1, source_target_pairs={{160,0},{128,32},{224,64},{192,96},{32,128},{0,160},{96,192},{64,2... | collective-permute-start | bytes 196616 | tf_op jit(solution)/shard_map/ppermute | solution.py:176
  101.5 1.0 collective-permute-start.8
  102.5 1.7 %collective-permute-start.9 = (bf16[64,512]{1,0:T(8,128)(2,1)S(1)}, bf16[64,512]{1,0:T(8,128)(2,1)S(1)}, u32[]{:S(2)}, u32[]{:S(2)}) collective-permute-start(bf16[64,512]{1,0:T(8,128)(2,1)S(1)} %get-tuple-element.20), channel_id=1, source_target_pairs={{224,0},{64,32},{32,64},{128,96},{96,128},{192,160},{160,192},{0,2... | collective-permute-start | bytes 196616 | tf_op jit(solution)/shard_map/ppermute | solution.py:176
  104.3 4.5 %collective-permute-done.7 = bf16[64,512]{1,0:T(8,128)(2,1)S(1)} collective-permute-done((bf16[64,512]{1,0:T(8,128)(2,1)S(1)}, bf16[64,512]{1,0:T(8,128)(2,1)S(1)}, u32[]{:S(2)}, u32[]{:S(2)}) %collective-permute-start.7) | collective-permute-done | bytes 65568 | tf_op jit(solution)/shard_map/ppermute | solution.py:176
  108.7 0.0 collective-permute-done.8
  108.7 0.5 collective-permute-done.9
  109.2 0.7 add_convert_fusion
Async XLA Ops:
  0.0 1.5 %collective-permute-start = (bf16[64,512]{1,0:T(8,128)(2,1)}, bf16[64,512]{1,0:T(8,128)(2,1)S(1)}, u32[]{:S(2)}, u32[]{:S(2)}) collective-permute-start(bf16[64,512]{1,0:T(8,128)(2,1)} %own_ref.1), channel_id=1, source_target_pairs={{0,1},{1,0},{2,3},{3,2},{4,5},{5,4},{6,7},{7,6},{8,9},{9,8},{10,11... | collective-permute-start | bytes 196616 | tf_op jit(solution)/shard_map/ppermute | solution.py:171
  1.5 0.9 copy-start.4
  2.5 8.4 %collective-permute-start.3 = (bf16[72,512]{1,0:T(8,128)(2,1)S(1)}, bf16[72,512]{1,0:T(8,128)(2,1)S(1)}, u32[]{:S(2)}, u32[]{:S(2)}) collective-permute-start(bf16[72,512]{1,0:T(8,128)(2,1)S(1)} %shard_map.74.own_ref), channel_id=1, source_target_pairs={{0,224},{32,64},{64,32},{96,128},{128,96},{160,192},{192,160},{224... | collective-permute-start | bytes 221192 | tf_op jit(solution)/shard_map/ppermute | solution.py:176
  4.5 7.1 %collective-permute-start.2 = (bf16[72,512]{1,0:T(8,128)(2,1)S(1)}, bf16[72,512]{1,0:T(8,128)(2,1)S(1)}, u32[]{:S(2)}, u32[]{:S(2)}) collective-permute-start(bf16[72,512]{1,0:T(8,128)(2,1)S(1)} %shard_map.74.own_ref), channel_id=1, source_target_pairs={{0,64},{32,224},{64,128},{96,32},{128,192},{160,96},{192,0},{224,1... | collective-permute-start | bytes 221192 | tf_op jit(solution)/shard_map/ppermute | solution.py:176
  8.1 10.0 %collective-permute-start.1 = (bf16[72,512]{1,0:T(8,128)(2,1)S(1)}, bf16[72,512]{1,0:T(8,128)(2,1)S(1)}, u32[]{:S(2)}, u32[]{:S(2)}) collective-permute-start(bf16[72,512]{1,0:T(8,128)(2,1)S(1)} %shard_map.74.own_ref), channel_id=1, source_target_pairs={{0,160},{32,128},{64,224},{96,192},{128,32},{160,0},{192,96},{224,... | collective-permute-start | bytes 221192 | tf_op jit(solution)/shard_map/ppermute | solution.py:176
  18.9 1.3 %copy-start = (bf16[32,64,512]{2,1,0:T(8,128)(2,1)}, bf16[32,64,512]{2,1,0:T(8,128)(2,1)S(1)}, u32[]{:S(2)}) copy-start(bf16[32,64,512]{2,1,0:T(8,128)(2,1)S(1)} %get-tuple-element.14) | copy-start | bytes 6291460
  20.2 9.2 %copy-start.1 = (bf16[2,1024,256]{2,1,0:T(8,128)(2,1)S(1)}, bf16[2,1024,256]{2,1,0:T(8,128)(2,1)}, u32[]{:S(2)}) copy-start(bf16[2,1024,256]{2,1,0:T(8,128)(2,1)} %gate_ref.1) | copy-start | bytes 3145732
  20.2 36.4 %all-to-all-start = ((bf16[64,32,512]{2,1,0:T(8,128)(2,1)}), bf16[64,32,512]{2,1,0:T(8,128)(2,1)S(1)}, u32[]{:S(2)}, u32[]{:S(2)}) async-start(bf16[64,32,512]{2,1,0:T(8,128)(2,1)} %bitcast.13), calls=%async_computation | async-start | bytes 4194304 | tf_op jit(solution)/shard_map/all_to_all | solution.py:179
  29.4 29.8 %collective-permute-start.4 = (bf16[2,1024,256]{2,1,0:T(8,128)(2,1)S(1)}, bf16[2,1024,256]{2,1,0:T(8,128)(2,1)}, u32[]{:S(2)}, u32[]{:S(2)}) collective-permute-start(bf16[2,1024,256]{2,1,0:T(8,128)(2,1)S(1)} %copy-done.1), channel_id=1, source_target_pairs={{0,1},{1,0},{2,3},{3,2},{4,5},{5,4},{6,7},{7,6},{8,9},{9,8},{10,11... | collective-permute-start | bytes 3145736 | tf_op jit(solution)/shard_map/ppermute | solution.py:171
  29.6 29.6 %collective-permute-start.5 = (bf16[2,1024,256]{2,1,0:T(8,128)(2,1)}, bf16[2,1024,256]{2,1,0:T(8,128)(2,1)}, u32[]{:S(2)}, u32[]{:S(2)}) collective-permute-start(bf16[2,1024,256]{2,1,0:T(8,128)(2,1)} %up_ref.1), channel_id=1, source_target_pairs={{0,1},{1,0},{2,3},{3,2},{4,5},{5,4},{6,7},{7,6},{8,9},{9,8},{10,11... | collective-permute-start | bytes 3145736 | tf_op jit(solution)/shard_map/ppermute | solution.py:171
  30.0 29.2 %collective-permute-start.6 = (bf16[2,512,512]{2,1,0:T(8,128)(2,1)}, bf16[2,512,512]{2,1,0:T(8,128)(2,1)}, u32[]{:S(2)}, u32[]{:S(2)}) collective-permute-start(bf16[2,512,512]{2,1,0:T(8,128)(2,1)} %down_ref.1), channel_id=1, source_target_pairs={{0,1},{1,0},{2,3},{3,2},{4,5},{5,4},{6,7},{7,6},{8,9},{9,8},{10,11... | collective-permute-start | bytes 3145736 | tf_op jit(solution)/shard_map/ppermute | solution.py:171
  56.7 1.2 %copy-start.2 = (bf16[2,1024,256]{2,1,0:T(8,128)(2,1)S(1)}, bf16[2,1024,256]{2,1,0:T(8,128)(2,1)}, u32[]{:S(2)}) copy-start(bf16[2,1024,256]{2,1,0:T(8,128)(2,1)} %up_ref.1) | copy-start | bytes 3145732
  57.9 1.3 %copy-start.3 = (bf16[2,512,512]{2,1,0:T(8,128)(2,1)S(1)}, bf16[2,512,512]{2,1,0:T(8,128)(2,1)}, u32[]{:S(2)}) copy-start(bf16[2,512,512]{2,1,0:T(8,128)(2,1)} %down_ref.1) | copy-start | bytes 3145732
  99.3 9.5 %collective-permute-start.7 = (bf16[64,512]{1,0:T(8,128)(2,1)S(1)}, bf16[64,512]{1,0:T(8,128)(2,1)S(1)}, u32[]{:S(2)}, u32[]{:S(2)}) collective-permute-start(bf16[64,512]{1,0:T(8,128)(2,1)S(1)} %get-tuple-element.18), channel_id=1, source_target_pairs={{160,0},{128,32},{224,64},{192,96},{32,128},{0,160},{96,192},{64,2... | collective-permute-start | bytes 196616 | tf_op jit(solution)/shard_map/ppermute | solution.py:176
  101.5 7.2 %collective-permute-start.8 = (bf16[64,512]{1,0:T(8,128)(2,1)S(1)}, bf16[64,512]{1,0:T(8,128)(2,1)S(1)}, u32[]{:S(2)}, u32[]{:S(2)}) collective-permute-start(bf16[64,512]{1,0:T(8,128)(2,1)S(1)} %get-tuple-element.19), channel_id=1, source_target_pairs={{64,0},{224,32},{128,64},{32,96},{192,128},{96,160},{0,192},{160,2... | collective-permute-start | bytes 196616 | tf_op jit(solution)/shard_map/ppermute | solution.py:176
  102.5 6.7 %collective-permute-start.9 = (bf16[64,512]{1,0:T(8,128)(2,1)S(1)}, bf16[64,512]{1,0:T(8,128)(2,1)S(1)}, u32[]{:S(2)}, u32[]{:S(2)}) collective-permute-start(bf16[64,512]{1,0:T(8,128)(2,1)S(1)} %get-tuple-element.20), channel_id=1, source_target_pairs={{224,0},{64,32},{32,64},{128,96},{96,128},{192,160},{160,192},{0,2... | collective-permute-start | bytes 196616 | tf_op jit(solution)/shard_map/ppermute | solution.py:176

commit v5 on v3

--- a/solution.py
+++ b/solution.py
@@ -62,7 +62,7 @@
 def place_pair(pair, place_ref, a_ref, b_ref, out_ref, table_ref):
     rows = a_ref.shape[0] - INFO
     span = 2 * rows
-    peers, block, half = out_ref.shape
+    _, peers, _, half = out_ref.shape
     experts = 2 * peers
     earlier = one_hot(
         (iota((span, span), 0) < iota((span, span), 1))
@@ -81,10 +81,10 @@
         slots.append(jnp.where((pick >= 0) & (pick < experts), slot, -1))
         weights.append(info[2 + k : 3 + k] + info[4 + k : 5 + k] + info[6 + k : 7 + k])
     for local in range(2):
-        at = local * (block // 2) + 16 * pair
+        at = 16 * pair
         slot = iota((16 * peers, span), 0) + local * 16 * peers
         sent = dot(one_hot((slot == slots[0]) | (slot == slots[1])), tokens)
-        out_ref[:, at : at + 16, :] = sent.astype(BF16).reshape(peers, 16, half)
+        out_ref[local, :, at : at + 16, :] = sent.astype(BF16).reshape(peers, 16, half)
     columns = [slot.astype(F32) for slot in slots] + weights
     table_ref[...] = jnp.concatenate(columns + columns, axis=0).T
 
@@ -94,20 +94,20 @@
 
 def hidden_part(rows_ref, at, gate_ref, up_ref, core):
     _, _, block, half = rows_ref.shape
-    low, high = (rows_ref[at : at + STEP // block, side].reshape(STEP, half) for side in range(2))
+    low, high = (rows_ref[side, at : at + STEP // block].reshape(STEP, half) for side in range(2))
     gate, up = (dot(low, ref[core, 0:half, :]) + dot(high, ref[core, half:, :]) for ref in (gate_ref, up_ref))
     return (gate / (1.0 + jnp.exp(-gate)) * up).astype(BF16)
 
 
 def own_kernel(place_ref, rows_ref, gate_ref, up_ref, out_ref):
-    chips, _, block, _ = rows_ref.shape
+    _, chips, block, _ = rows_ref.shape
     for at in range(0, chips, STEP // block):
         out_ref[at * block : at * block + STEP] = hidden_part(rows_ref, at, gate_ref, up_ref, place_ref[0] % 2)
 
 
 def expert_kernel(place_ref, rows_ref, own_ref, gate2_ref, up2_ref, down_ref, down2_ref, out_ref):
     core = place_ref[0] % 2
-    chips, _, block, half = rows_ref.shape
+    _, chips, block, half = rows_ref.shape
     width = own_ref.shape[1]
     sides = (core, 1 - core)
     spans = [pl.ds(pl.multiple_of(side * width, width), width) for side in sides]
@@ -117,16 +117,16 @@
         other = hidden_part(rows_ref, at, gate2_ref, up2_ref, core)
         for side, down in zip(sides, (down_ref, down2_ref)):
             result = dot(own, down[core, spans[0], :]) + dot(other, down[core, spans[1], :])
-            out_ref[at : at + step, side] = result.astype(BF16).reshape(step, block, half)
+            out_ref[side, at : at + step] = result.astype(BF16).reshape(step, block, half)
 
 
 def combine_kernel(pair, back_ref, table_ref, a_ref, b_ref):
     rows, half = a_ref.shape
-    peers, block, _ = back_ref.shape
+    _, peers, _, _ = back_ref.shape
     picked = None
     for local in range(2):
-        at = local * (block // 2) + 16 * pair
-        back = back_ref[:, at : at + 16, :].reshape(16 * peers, half)
+        at = 16 * pair
+        back = back_ref[local, :, at : at + 16, :].reshape(16 * peers, half)
         place = iota((2 * rows, 16 * peers), 1) + local * 16 * peers
         chosen = [one_hot(place == table_ref[:, k : k + 1].astype(jnp.int32)) for k in range(2)]
         term = dot(jnp.concatenate(chosen, axis=0), back)
@@ -154,7 +154,7 @@
 def local(tokens, norm_gain, routing, route_weight, w_gate, w_up, w_down):
     rows, half = tokens.shape
     columns = lax.axis_size("zh")
-    plane = ("zl", "y", "x", "tp")
+    plane = ("tp", "zl", "y", "x")
     peers = lax.axis_size(plane) // 2
     experts, _, width = w_gate.shape
     block = experts * columns * CAP
@@ -186,14 +186,14 @@
     first = relay(own, -1)
     second = relay(own, 2)
 
-    buffer = jax.ShapeDtypeStruct((peers, block, half), BF16)
+    buffer = jax.ShapeDtypeStruct((2, peers, block // 2, half), BF16)
     small = jax.ShapeDtypeStruct((2 * rows, 8), F32)
     flops = total * 2 * rows * half
     sent, table0, table1 = call(
         dispatch_kernel, (buffer, small, small), (place, own, first, third, second), 2 * flops, 12, 1
     )
     arrived = exchange(sent.reshape(2 * peers, block // 2, half), plane)
-    arrived = arrived.reshape(peers, 2, block // 2, half)
+    arrived = arrived.reshape(2, peers, block // 2, half)
     hidden = call(
         own_kernel,
         jax.ShapeDtypeStruct((total // 2, width), BF16),
@@ -204,14 +204,14 @@
     )
     result = call(
         expert_kernel,
-        jax.ShapeDtypeStruct((peers, 2, block // 2, half), BF16),
+        buffer,
         (place, arrived, hidden, gate2, up2, w_down, down2),
         total * half * width * 8,
         16,
         1,
     )
     back = exchange(result.reshape(2 * peers, block // 2, half), plane)
-    back = back.reshape(peers, block, half)
+    back = back.reshape(2, peers, block // 2, half)
     pair = (jax.ShapeDtypeStruct((rows, half), BF16),) * 2
     third, second = call(functools.partial(combine_kernel, 1), pair, (back, table1), 2 * flops, 8)
     home = [relay(third, -3, home=True)]

time: 111 us -> 112 us (level)
    all_to_all x1, waiting for transfers between devices: 26.5 us -> 27.7 us  [exchange(): return lax.all_to_all(v, axes, split_axis=0, concat_axis=0, tiled=True)]
where the time goes in v5:
time: 112 us; the launch traced here: 110 us
  waiting for transfers between devices  38.4 us (34%)
  blocking collectives  34.3 us (31%)
  starting transfers between devices  24 us (21%)
  Pallas kernels  9.17 us (8%)
  local copies, waits for them, and re-layouts  3.45 us (3%)
    all_to_all x1, blocking collectives, exchange(): return lax.all_to_all(v, axes, split_axis=0, concat_axis=0, tiled=True)  34.3 us
    all_to_all x1, waiting for transfers between devices, exchange(): return lax.all_to_all(v, axes, split_axis=0, concat_axis=0, tiled=True)  27.7 us
    ppermute x6, starting transfers between devices, relay(): lax.ppermute(v, ('zh', 'zl'), [(to, z) for z, to in pairs] if home else p...  14 us
    ppermute x6, waiting for transfers between devices, relay(): lax.ppermute(v, ('zh', 'zl'), [(to, z) for z, to in pairs] if home else p...  10.7 us
    pallas_call x7, Pallas kernels, call(): pl.pallas_call(kernel, out_shape=out_shape, cost_estimate=pl.CostEstimate...  9.17 us
    all_to_all x1, starting transfers between devices, exchange(): return lax.all_to_all(v, axes, split_axis=0, concat_axis=0, tiled=True)  9.1 us
    unnamed x10, local copies, waits for them, and re-layouts  3.45 us
  transfers between devices with their start and end apart: 11, of which 5 were waited for; matrix products, arithmetic and copies ran while one was open for 0% of the time, Pallas kernels for 3%

profile of v5, /device:TPU:32, one launch (start us, length us, event | category | flops | bytes accessed | tf_op | source)
XLA Modules:
  0.0 110.1 jit_solution(16424491889874037758)
XLA Ops:
  0.0 0.0 collective-permute-start
  0.0 1.5 %shard_map.73.held_ref = bf16[80,512]{1,0:T(8,128)(2,1)} custom-call(bf16[64,512]{1,0:T(8,128)(2,1)} %own_ref.1, f32[1,512]{1,0:T(1,128)} %bitcast.14, s32[2,64]{1,0:T(2,128)} %bitcast.15, f32[2,64]{1,0:T(2,128)} %bitcast.16), custom_call_target="tpu_custom_call" | custom-call | flops 32768 | bytes 68608 | tf_op jit(solution)/shard_map/pallas_call | solution.py:145
  1.5 0.0 collective-permute-done.other_ref
  1.5 0.0 copy-start.4
  1.5 0.9 copy-done.4
  2.4 0.1 shard_map.74.own_ref
  2.5 5.5 %collective-permute-start.3 = (bf16[72,512]{1,0:T(8,128)(2,1)S(1)}, bf16[72,512]{1,0:T(8,128)(2,1)S(1)}, u32[]{:S(2)}, u32[]{:S(2)}) collective-permute-start(bf16[72,512]{1,0:T(8,128)(2,1)S(1)} %shard_map.74.own_ref), channel_id=1, source_target_pairs={{0,64},{32,224},{64,128},{96,32},{128,192},{160,96},{192,0},{224,1... | collective-permute-start | bytes 221192 | tf_op jit(solution)/shard_map/ppermute | solution.py:170
  8.0 1.9 %collective-permute-start.2 = (bf16[72,512]{1,0:T(8,128)(2,1)S(1)}, bf16[72,512]{1,0:T(8,128)(2,1)S(1)}, u32[]{:S(2)}, u32[]{:S(2)}) collective-permute-start(bf16[72,512]{1,0:T(8,128)(2,1)S(1)} %shard_map.74.own_ref), channel_id=1, source_target_pairs={{0,160},{32,128},{64,224},{96,192},{128,32},{160,0},{192,96},{224,... | collective-permute-start | bytes 221192 | tf_op jit(solution)/shard_map/ppermute | solution.py:170
  9.9 1.0 collective-permute-start.1
  10.9 0.0 collective-permute-done.3.second_ref
  10.9 5.5 %collective-permute-done.2.third_ref = bf16[72,512]{1,0:T(8,128)(2,1)S(1)} collective-permute-done((bf16[72,512]{1,0:T(8,128)(2,1)S(1)}, bf16[72,512]{1,0:T(8,128)(2,1)S(1)}, u32[]{:S(2)}, u32[]{:S(2)}) %collective-permute-start.2) | collective-permute-done | bytes 73760 | tf_op jit(solution)/shard_map/ppermute | solution.py:170
  16.4 0.0 collective-permute-done.1.first_ref
  16.5 1.0 shard_map.75
  17.5 0.0 copy-start
  17.5 1.3 %copy-done = bf16[2,32,32,512]{3,2,1,0:T(8,128)(2,1)} copy-done((bf16[2,32,32,512]{3,2,1,0:T(8,128)(2,1)}, bf16[2,32,32,512]{3,2,1,0:T(8,128)(2,1)S(1)}, u32[]{:S(2)}) %copy-start) | copy-done | bytes 2097176
  18.9 0.0 copy-start.1
  18.9 9.1 %all-to-all-start = ((bf16[64,32,512]{2,1,0:T(8,128)(2,1)}), bf16[64,32,512]{2,1,0:T(8,128)(2,1)S(1)}, u32[]{:S(2)}, u32[]{:S(2)}) async-start(bf16[64,32,512]{2,1,0:T(8,128)(2,1)} %bitcast.13), calls=%async_computation | async-start | bytes 4194304 | tf_op jit(solution)/shard_map/all_to_all | solution.py:173
  28.0 0.0 copy-done.1
  28.0 0.4 collective-permute-start.4
  28.4 0.2 collective-permute-start.5
  28.6 0.3 collective-permute-start.6
  28.9 27.7 %all-to-all-done = bf16[64,32,512]{2,1,0:T(8,128)(2,1)S(1)} async-done(((bf16[64,32,512]{2,1,0:T(8,128)(2,1)}), bf16[64,32,512]{2,1,0:T(8,128)(2,1)S(1)}, u32[]{:S(2)}, u32[]{:S(2)}) %all-to-all-start) | async-done | bytes 2097184 | tf_op jit(solution)/shard_map/all_to_all | solution.py:173
  56.6 0.0 copy-start.2
  56.6 1.2 %copy-done.2 = bf16[2,1024,256]{2,1,0:T(8,128)(2,1)S(1)} copy-done((bf16[2,1024,256]{2,1,0:T(8,128)(2,1)S(1)}, bf16[2,1024,256]{2,1,0:T(8,128)(2,1)}, u32[]{:S(2)}) %copy-start.2) | copy-done | bytes 1048600
  57.8 0.0 copy-start.3
  57.8 1.3 %shard_map.76.own_ref = bf16[1024,256]{1,0:T(8,128)(2,1)S(1)} custom-call(s32[1]{0:T(128)} %bitcast.place_ref, bf16[2,32,32,512]{3,2,1,0:T(8,128)(2,1)S(1)} %bitcast.8, bf16[2,1024,256]{2,1,0:T(8,128)(2,1)S(1)} %copy-done.1, bf16[2,1024,256]{2,1,0:T(8,128)(2,1)S(1)} %copy-done.2), custom_call_target="tpu_custom_call" | custom-call | flops 1073741824 | bytes 4194308 | tf_op jit(solution)/shard_map/pallas_call | solution.py:145
  59.1 0.0 collective-permute-done.4.gate2_ref
  59.1 0.0 collective-permute-done.5.up2_ref
  59.1 0.0 collective-permute-done.6.down2_ref
  59.1 0.0 copy-done.3
  59.1 4.2 %shard_map.77 = bf16[2,32,32,512]{3,2,1,0:T(8,128)(2,1)S(1)} custom-call(s32[1]{0:T(128)} %bitcast.place_ref, bf16[2,32,32,512]{3,2,1,0:T(8,128)(2,1)S(1)} %bitcast.9, bf16[1024,256]{1,0:T(8,128)(2,1)S(1)} %shard_map.76.own_ref, bf16[2,1024,256]{2,1,0:T(8,128)(2,1)} %collective-permute-done.4.gate2_ref, ...), custom_call_target="tpu_custom_call" | custom-call | flops 2147483648 | bytes 6815748 | tf_op jit(solution)/shard_map/pallas_call | solution.py:145
  63.3 34.3 %all_to_all.10 = bf16[64,32,512]{2,1,0:T(8,128)(2,1)S(1)} all-to-all(bf16[64,32,512]{2,1,0:T(8,128)(2,1)S(1)} %bitcast.12), channel_id=1, replica_groups=mesh['zh'=4,'zl'=2,'y'=4,'x'=4,'tp'=2] {'tp','zl','y','x'}, dimensions={0} | all-to-all | bytes 4194304 | tf_op jit(solution)/shard_map/all_to_all | solution.py:173
  97.7 0.5 shard_map.79
  98.2 0.5 shard_map.78
  98.7 2.5 %collective-permute-start.7 = (bf16[64,512]{1,0:T(8,128)(2,1)S(1)}, bf16[64,512]{1,0:T(8,128)(2,1)S(1)}, u32[]{:S(2)}, u32[]{:S(2)}) collective-permute-start(bf16[64,512]{1,0:T(8,128)(2,1)S(1)} %get-tuple-element.16), channel_id=1, source_target_pairs={{160,0},{128,32},{224,64},{192,96},{32,128},{0,160},{96,192},{64,2... | collective-permute-start | bytes 196616 | tf_op jit(solution)/shard_map/ppermute | solution.py:170
  101.2 1.9 %collective-permute-start.8 = (bf16[64,512]{1,0:T(8,128)(2,1)S(1)}, bf16[64,512]{1,0:T(8,128)(2,1)S(1)}, u32[]{:S(2)}, u32[]{:S(2)}) collective-permute-start(bf16[64,512]{1,0:T(8,128)(2,1)S(1)} %get-tuple-element.17), channel_id=1, source_target_pairs={{64,0},{224,32},{128,64},{32,96},{192,128},{96,160},{0,192},{160,2... | collective-permute-start | bytes 196616 | tf_op jit(solution)/shard_map/ppermute | solution.py:170
  103.2 1.1 %collective-permute-start.9 = (bf16[64,512]{1,0:T(8,128)(2,1)S(1)}, bf16[64,512]{1,0:T(8,128)(2,1)S(1)}, u32[]{:S(2)}, u32[]{:S(2)}) collective-permute-start(bf16[64,512]{1,0:T(8,128)(2,1)S(1)} %get-tuple-element.18), channel_id=1, source_target_pairs={{224,0},{64,32},{32,64},{128,96},{96,128},{192,160},{160,192},{0,2... | collective-permute-start | bytes 196616 | tf_op jit(solution)/shard_map/ppermute | solution.py:170
  104.3 2.7 %collective-permute-done.7 = bf16[64,512]{1,0:T(8,128)(2,1)S(1)} collective-permute-done((bf16[64,512]{1,0:T(8,128)(2,1)S(1)}, bf16[64,512]{1,0:T(8,128)(2,1)S(1)}, u32[]{:S(2)}, u32[]{:S(2)}) %collective-permute-start.7) | collective-permute-done | bytes 65568 | tf_op jit(solution)/shard_map/ppermute | solution.py:170
  107.0 1.9 %collective-permute-done.8 = bf16[64,512]{1,0:T(8,128)(2,1)S(1)} collective-permute-done((bf16[64,512]{1,0:T(8,128)(2,1)S(1)}, bf16[64,512]{1,0:T(8,128)(2,1)S(1)}, u32[]{:S(2)}, u32[]{:S(2)}) %collective-permute-start.8) | collective-permute-done | bytes 65568 | tf_op jit(solution)/shard_map/ppermute | solution.py:170
  108.8 0.7 collective-permute-done.9
  109.5 0.7 add_convert_fusion
Async XLA Ops:
  0.0 1.5 %collective-permute-start = (bf16[64,512]{1,0:T(8,128)(2,1)}, bf16[64,512]{1,0:T(8,128)(2,1)S(1)}, u32[]{:S(2)}, u32[]{:S(2)}) collective-permute-start(bf16[64,512]{1,0:T(8,128)(2,1)} %own_ref.1), channel_id=1, source_target_pairs={{0,1},{1,0},{2,3},{3,2},{4,5},{5,4},{6,7},{7,6},{8,9},{9,8},{10,11... | collective-permute-start | bytes 196616 | tf_op jit(solution)/shard_map/ppermute | solution.py:165
  1.5 0.9 copy-start.4
  2.5 8.4 %collective-permute-start.3 = (bf16[72,512]{1,0:T(8,128)(2,1)S(1)}, bf16[72,512]{1,0:T(8,128)(2,1)S(1)}, u32[]{:S(2)}, u32[]{:S(2)}) collective-permute-start(bf16[72,512]{1,0:T(8,128)(2,1)S(1)} %shard_map.74.own_ref), channel_id=1, source_target_pairs={{0,64},{32,224},{64,128},{96,32},{128,192},{160,96},{192,0},{224,1... | collective-permute-start | bytes 221192 | tf_op jit(solution)/shard_map/ppermute | solution.py:170
  8.0 8.4 %collective-permute-start.2 = (bf16[72,512]{1,0:T(8,128)(2,1)S(1)}, bf16[72,512]{1,0:T(8,128)(2,1)S(1)}, u32[]{:S(2)}, u32[]{:S(2)}) collective-permute-start(bf16[72,512]{1,0:T(8,128)(2,1)S(1)} %shard_map.74.own_ref), channel_id=1, source_target_pairs={{0,160},{32,128},{64,224},{96,192},{128,32},{160,0},{192,96},{224,... | collective-permute-start | bytes 221192 | tf_op jit(solution)/shard_map/ppermute | solution.py:170
  9.9 6.5 %collective-permute-start.1 = (bf16[72,512]{1,0:T(8,128)(2,1)S(1)}, bf16[72,512]{1,0:T(8,128)(2,1)S(1)}, u32[]{:S(2)}, u32[]{:S(2)}) collective-permute-start(bf16[72,512]{1,0:T(8,128)(2,1)S(1)} %shard_map.74.own_ref), channel_id=1, source_target_pairs={{0,224},{32,64},{64,32},{96,128},{128,96},{160,192},{192,160},{224... | collective-permute-start | bytes 221192 | tf_op jit(solution)/shard_map/ppermute | solution.py:170
  17.5 1.3 %copy-start = (bf16[2,32,32,512]{3,2,1,0:T(8,128)(2,1)}, bf16[2,32,32,512]{3,2,1,0:T(8,128)(2,1)S(1)}, u32[]{:S(2)}) copy-start(bf16[2,32,32,512]{3,2,1,0:T(8,128)(2,1)S(1)} %get-tuple-element.12) | copy-start | bytes 6291460
  18.9 9.1 %copy-start.1 = (bf16[2,1024,256]{2,1,0:T(8,128)(2,1)S(1)}, bf16[2,1024,256]{2,1,0:T(8,128)(2,1)}, u32[]{:S(2)}) copy-start(bf16[2,1024,256]{2,1,0:T(8,128)(2,1)} %gate_ref.1) | copy-start | bytes 3145732
  18.9 37.7 %all-to-all-start = ((bf16[64,32,512]{2,1,0:T(8,128)(2,1)}), bf16[64,32,512]{2,1,0:T(8,128)(2,1)S(1)}, u32[]{:S(2)}, u32[]{:S(2)}) async-start(bf16[64,32,512]{2,1,0:T(8,128)(2,1)} %bitcast.13), calls=%async_computation | async-start | bytes 4194304 | tf_op jit(solution)/shard_map/all_to_all | solution.py:173
  28.0 31.1 %collective-permute-start.4 = (bf16[2,1024,256]{2,1,0:T(8,128)(2,1)S(1)}, bf16[2,1024,256]{2,1,0:T(8,128)(2,1)}, u32[]{:S(2)}, u32[]{:S(2)}) collective-permute-start(bf16[2,1024,256]{2,1,0:T(8,128)(2,1)S(1)} %copy-done.1), channel_id=1, source_target_pairs={{0,1},{1,0},{2,3},{3,2},{4,5},{5,4},{6,7},{7,6},{8,9},{9,8},{10,11... | collective-permute-start | bytes 3145736 | tf_op jit(solution)/shard_map/ppermute | solution.py:165
  28.4 30.7 %collective-permute-start.5 = (bf16[2,1024,256]{2,1,0:T(8,128)(2,1)}, bf16[2,1024,256]{2,1,0:T(8,128)(2,1)}, u32[]{:S(2)}, u32[]{:S(2)}) collective-permute-start(bf16[2,1024,256]{2,1,0:T(8,128)(2,1)} %up_ref.1), channel_id=1, source_target_pairs={{0,1},{1,0},{2,3},{3,2},{4,5},{5,4},{6,7},{7,6},{8,9},{9,8},{10,11... | collective-permute-start | bytes 3145736 | tf_op jit(solution)/shard_map/ppermute | solution.py:165
  28.6 30.5 %collective-permute-start.6 = (bf16[2,512,512]{2,1,0:T(8,128)(2,1)}, bf16[2,512,512]{2,1,0:T(8,128)(2,1)}, u32[]{:S(2)}, u32[]{:S(2)}) collective-permute-start(bf16[2,512,512]{2,1,0:T(8,128)(2,1)} %down_ref.1), channel_id=1, source_target_pairs={{0,1},{1,0},{2,3},{3,2},{4,5},{5,4},{6,7},{7,6},{8,9},{9,8},{10,11... | collective-permute-start | bytes 3145736 | tf_op jit(solution)/shard_map/ppermute | solution.py:165
  56.6 1.2 %copy-start.2 = (bf16[2,1024,256]{2,1,0:T(8,128)(2,1)S(1)}, bf16[2,1024,256]{2,1,0:T(8,128)(2,1)}, u32[]{:S(2)}) copy-start(bf16[2,1024,256]{2,1,0:T(8,128)(2,1)} %up_ref.1) | copy-start | bytes 3145732
  57.8 1.3 %copy-start.3 = (bf16[2,512,512]{2,1,0:T(8,128)(2,1)S(1)}, bf16[2,512,512]{2,1,0:T(8,128)(2,1)}, u32[]{:S(2)}) copy-start(bf16[2,512,512]{2,1,0:T(8,128)(2,1)} %down_ref.1) | copy-start | bytes 3145732
  98.7 8.3 %collective-permute-start.7 = (bf16[64,512]{1,0:T(8,128)(2,1)S(1)}, bf16[64,512]{1,0:T(8,128)(2,1)S(1)}, u32[]{:S(2)}, u32[]{:S(2)}) collective-permute-start(bf16[64,512]{1,0:T(8,128)(2,1)S(1)} %get-tuple-element.16), channel_id=1, source_target_pairs={{160,0},{128,32},{224,64},{192,96},{32,128},{0,160},{96,192},{64,2... | collective-permute-start | bytes 196616 | tf_op jit(solution)/shard_map/ppermute | solution.py:170
  101.2 7.6 %collective-permute-start.8 = (bf16[64,512]{1,0:T(8,128)(2,1)S(1)}, bf16[64,512]{1,0:T(8,128)(2,1)S(1)}, u32[]{:S(2)}, u32[]{:S(2)}) collective-permute-start(bf16[64,512]{1,0:T(8,128)(2,1)S(1)} %get-tuple-element.17), channel_id=1, source_target_pairs={{64,0},{224,32},{128,64},{32,96},{192,128},{96,160},{0,192},{160,2... | collective-permute-start | bytes 196616 | tf_op jit(solution)/shard_map/ppermute | solution.py:170
  103.2 6.3 %collective-permute-start.9 = (bf16[64,512]{1,0:T(8,128)(2,1)S(1)}, bf16[64,512]{1,0:T(8,128)(2,1)S(1)}, u32[]{:S(2)}, u32[]{:S(2)}) collective-permute-start(bf16[64,512]{1,0:T(8,128)(2,1)S(1)} %get-tuple-element.18), channel_id=1, source_target_pairs={{224,0},{64,32},{32,64},{128,96},{96,128},{192,160},{160,192},{0,2... | collective-permute-start | bytes 196616 | tf_op jit(solution)/shard_map/ppermute | solution.py:170

commit v6 on v4

--- a/solution.py
+++ b/solution.py
@@ -126,21 +126,22 @@
             out_ref[at : at + step, side] = result.astype(BF16).reshape(step, block, half)
 
 
-def combine_kernel(pair, back_ref, table_ref, a_ref, b_ref):
-    rows, half = a_ref.shape
+def combine_kernel(pair, side, back_ref, table_ref, *out_refs):
+    rows, half = out_refs[0].shape
     peers, block, _ = back_ref.shape
+    span = rows * len(out_refs)
+    table = table_ref[side * rows : side * rows + span, :]
     picked = None
     for local in range(2):
         at = local * (block // 2) + 16 * pair
         back = back_ref[:, at : at + 16, :].reshape(16 * peers, half)
-        place = iota((2 * rows, 16 * peers), 1) + local * 16 * peers
-        chosen = [one_hot(place == table_ref[:, k : k + 1].astype(jnp.int32)) for k in range(2)]
+        place = iota((span, 16 * peers), 1) + local * 16 * peers
+        chosen = [one_hot(place == table[:, k : k + 1].astype(jnp.int32)) for k in range(2)]
         term = dot(jnp.concatenate(chosen, axis=0), back)
         picked = term if picked is None else picked + term
-    total = picked[0 : 2 * rows] * table_ref[:, 2:3] + picked[2 * rows :] * table_ref[:, 3:4]
-    total = total.astype(BF16)
-    a_ref[...] = total[0:rows]
-    b_ref[...] = total[rows:]
+    total = (picked[0:span] * table[:, 2:3] + picked[span:] * table[:, 3:4]).astype(BF16)
+    for i, out_ref in enumerate(out_refs):
+        out_ref[...] = total[i * rows : (i + 1) * rows]
 
 
 def call(kernel, out_shape, args, flops, grant, scalars=0, **kw):
@@ -224,11 +225,12 @@
     )
     back = exchange(result.reshape(2 * peers, block // 2, half), plane)
     back = back.reshape(peers, block, half)
-    pair = (jax.ShapeDtypeStruct((rows, half), BF16),) * 2
-    third, second = call(functools.partial(combine_kernel, 1), pair, (back, table1), 2 * flops, 8)
+    one = jax.ShapeDtypeStruct((rows, half), BF16)
+    third = call(functools.partial(combine_kernel, 1, 0), one, (back, table1), flops, 8)
     home = [relay(third, -3, home=True)]
+    second = call(functools.partial(combine_kernel, 1, 1), one, (back, table1), flops, 8)
     home += [relay(second, 2, home=True)]
-    own, first = call(functools.partial(combine_kernel, 0), pair, (back, table0), 2 * flops, 8)
+    own, first = call(functools.partial(combine_kernel, 0, 0), (one, one), (back, table0), 2 * flops, 8)
     home += [relay(first, -1, home=True)]
     return sum((part.astype(F32) for part in home), own.astype(F32)).astype(BF16)
 

time: 112 us -> 112 us (level)
    pallas_call x8 -> x9, Pallas kernels: 9.48 us -> 9.68 us  [call(): pl.pallas_call(kernel, out_shape=out_shape, cost_estimate=pl.CostEstimate...]
where the time goes in v6:
time: 112 us; the launch traced here: 111 us
  waiting for transfers between devices  38.9 us (35%)
  blocking collectives  34.8 us (31%)
  starting transfers between devices  23.3 us (21%)
  Pallas kernels  9.68 us (9%)
  local copies, waits for them, and re-layouts  3.46 us (3%)
    all_to_all x1, blocking collectives, exchange(): return lax.all_to_all(v, axes, split_axis=0, concat_axis=0, tiled=True)  34.8 us
    all_to_all x1, waiting for transfers between devices, exchange(): return lax.all_to_all(v, axes, split_axis=0, concat_axis=0, tiled=True)  26.5 us
    ppermute x6, starting transfers between devices, relay(): lax.ppermute(v, ('zh', 'zl'), [(to, z) for z, to in pairs] if home else p...  13.4 us
    ppermute x6, waiting for transfers between devices, relay(): lax.ppermute(v, ('zh', 'zl'), [(to, z) for z, to in pairs] if home else p...  12.3 us
    pallas_call x9, Pallas kernels, call(): pl.pallas_call(kernel, out_shape=out_shape, cost_estimate=pl.CostEstimate...  9.68 us
    all_to_all x1, starting transfers between devices, exchange(): return lax.all_to_all(v, axes, split_axis=0, concat_axis=0, tiled=True)  9.17 us
    unnamed x10, local copies, waits for them, and re-layouts  3.46 us
  transfers between devices with their start and end apart: 11, of which 5 were waited for; matrix products, arithmetic and copies ran while one was open for 0% of the time, Pallas kernels for 3%

profile of v6, /device:TPU:32, one launch (start us, length us, event | category | flops | bytes accessed | tf_op | source)
XLA Modules:
  0.0 110.9 jit_solution(15857209722442696782)
XLA Ops:
  0.0 0.0 collective-permute-start
  0.0 1.5 %shard_map.73.held_ref = bf16[80,512]{1,0:T(8,128)(2,1)} custom-call(bf16[64,512]{1,0:T(8,128)(2,1)} %own_ref.1, f32[1,512]{1,0:T(1,128)} %bitcast.15, s32[2,64]{1,0:T(2,128)} %bitcast.16, f32[2,64]{1,0:T(2,128)} %bitcast.17), custom_call_target="tpu_custom_call" | custom-call | flops 32768 | bytes 68608 | tf_op jit(solution)/shard_map/pallas_call | solution.py:152
  1.5 0.0 collective-permute-done.other_ref
  1.5 0.0 copy-start.4
  1.5 0.9 copy-done.4
  2.4 0.1 shard_map.74.own_ref
  2.5 2.0 %collective-permute-start.3 = (bf16[72,512]{1,0:T(8,128)(2,1)S(1)}, bf16[72,512]{1,0:T(8,128)(2,1)S(1)}, u32[]{:S(2)}, u32[]{:S(2)}) collective-permute-start(bf16[72,512]{1,0:T(8,128)(2,1)S(1)} %shard_map.74.own_ref), channel_id=1, source_target_pairs={{0,224},{32,64},{64,32},{96,128},{128,96},{160,192},{192,160},{224... | collective-permute-start | bytes 221192 | tf_op jit(solution)/shard_map/ppermute | solution.py:177
  4.5 3.6 %collective-permute-start.2 = (bf16[72,512]{1,0:T(8,128)(2,1)S(1)}, bf16[72,512]{1,0:T(8,128)(2,1)S(1)}, u32[]{:S(2)}, u32[]{:S(2)}) collective-permute-start(bf16[72,512]{1,0:T(8,128)(2,1)S(1)} %shard_map.74.own_ref), channel_id=1, source_target_pairs={{0,64},{32,224},{64,128},{96,32},{128,192},{160,96},{192,0},{224,1... | collective-permute-start | bytes 221192 | tf_op jit(solution)/shard_map/ppermute | solution.py:177
  8.1 2.8 %collective-permute-start.1 = (bf16[72,512]{1,0:T(8,128)(2,1)S(1)}, bf16[72,512]{1,0:T(8,128)(2,1)S(1)}, u32[]{:S(2)}, u32[]{:S(2)}) collective-permute-start(bf16[72,512]{1,0:T(8,128)(2,1)S(1)} %shard_map.74.own_ref), channel_id=1, source_target_pairs={{0,160},{32,128},{64,224},{96,192},{128,32},{160,0},{192,96},{224,... | collective-permute-start | bytes 221192 | tf_op jit(solution)/shard_map/ppermute | solution.py:177
  10.9 0.0 collective-permute-done.3.first_ref
  10.9 0.6 shard_map.75
  11.6 0.1 collective-permute-done.2.second_ref
  11.7 6.4 %collective-permute-done.1.third_ref = bf16[72,512]{1,0:T(8,128)(2,1)S(1)} collective-permute-done((bf16[72,512]{1,0:T(8,128)(2,1)S(1)}, bf16[72,512]{1,0:T(8,128)(2,1)S(1)}, u32[]{:S(2)}, u32[]{:S(2)}) %collective-permute-start.1) | collective-permute-done | bytes 73760 | tf_op jit(solution)/shard_map/ppermute | solution.py:177
  18.1 0.7 shard_map.76
  18.9 0.0 copy-start
  18.9 1.3 %copy-done = bf16[32,64,512]{2,1,0:T(8,128)(2,1)} copy-done((bf16[32,64,512]{2,1,0:T(8,128)(2,1)}, bf16[32,64,512]{2,1,0:T(8,128)(2,1)S(1)}, u32[]{:S(2)}) %copy-start) | copy-done | bytes 2097176
  20.2 0.0 copy-start.1
  20.2 9.2 %all-to-all-start = ((bf16[64,32,512]{2,1,0:T(8,128)(2,1)}), bf16[64,32,512]{2,1,0:T(8,128)(2,1)S(1)}, u32[]{:S(2)}, u32[]{:S(2)}) async-start(bf16[64,32,512]{2,1,0:T(8,128)(2,1)} %bitcast.14), calls=%async_computation | async-start | bytes 4194304 | tf_op jit(solution)/shard_map/all_to_all | solution.py:180
  29.4 0.0 copy-done.1
  29.4 0.2 collective-permute-start.4
  29.6 0.4 collective-permute-start.5
  30.0 0.1 collective-permute-start.6
  30.1 26.5 %all-to-all-done = bf16[64,32,512]{2,1,0:T(8,128)(2,1)S(1)} async-done(((bf16[64,32,512]{2,1,0:T(8,128)(2,1)}), bf16[64,32,512]{2,1,0:T(8,128)(2,1)S(1)}, u32[]{:S(2)}, u32[]{:S(2)}) %all-to-all-start) | async-done | bytes 2097184 | tf_op jit(solution)/shard_map/all_to_all | solution.py:180
  56.7 0.0 copy-start.2
  56.7 1.2 %copy-done.2 = bf16[2,1024,256]{2,1,0:T(8,128)(2,1)S(1)} copy-done((bf16[2,1024,256]{2,1,0:T(8,128)(2,1)S(1)}, bf16[2,1024,256]{2,1,0:T(8,128)(2,1)}, u32[]{:S(2)}) %copy-start.2) | copy-done | bytes 1048600
  57.9 0.0 copy-start.3
  57.9 1.3 %shard_map.77.own_ref = bf16[1024,256]{1,0:T(8,128)(2,1)S(1)} custom-call(s32[1]{0:T(128)} %bitcast.place_ref, bf16[32,2,32,512]{3,2,1,0:T(8,128)(2,1)S(1)} %bitcast.11, bf16[2,1024,256]{2,1,0:T(8,128)(2,1)S(1)} %copy-done.1, bf16[2,1024,256]{2,1,0:T(8,128)(2,1)S(1)} %copy-done.2), custom_call_target="tpu_custom_call" | custom-call | flops 1073741824 | bytes 4194308 | tf_op jit(solution)/shard_map/pallas_call | solution.py:152
  59.2 0.0 collective-permute-done.4.gate2_ref
  59.2 0.0 collective-permute-done.5.up2_ref
  59.2 0.0 collective-permute-done.6.down2_ref
  59.2 0.0 copy-done.3
  59.2 4.2 %shard_map.78 = bf16[32,2,32,512]{3,2,1,0:T(8,128)(2,1)S(1)} custom-call(s32[1]{0:T(128)} %bitcast.place_ref, bf16[32,2,32,512]{3,2,1,0:T(8,128)(2,1)S(1)} %bitcast.12, bf16[1024,256]{1,0:T(8,128)(2,1)S(1)} %shard_map.77.own_ref, bf16[2,1024,256]{2,1,0:T(8,128)(2,1)} %collective-permute-done.4.gate2_ref, ...), custom_call_target="tpu_custom_call" | custom-call | flops 2147483648 | bytes 6815748 | tf_op jit(solution)/shard_map/pallas_call | solution.py:152
  63.4 34.8 %all_to_all.10 = bf16[64,32,512]{2,1,0:T(8,128)(2,1)S(1)} all-to-all(bf16[64,32,512]{2,1,0:T(8,128)(2,1)S(1)} %bitcast.13), channel_id=1, replica_groups=mesh['zh'=4,'zl'=2,'y'=4,'x'=4,'tp'=2] {'zl','y','x','tp'}, dimensions={0} | all-to-all | bytes 4194304 | tf_op jit(solution)/shard_map/all_to_all | solution.py:180
  98.3 0.4 shard_map.81
  98.6 0.4 shard_map.80
  99.0 0.5 shard_map.79
  99.5 0.4 collective-permute-start.9
  99.9 3.4 %collective-permute-start.7 = (bf16[64,512]{1,0:T(8,128)(2,1)S(1)}, bf16[64,512]{1,0:T(8,128)(2,1)S(1)}, u32[]{:S(2)}, u32[]{:S(2)}) collective-permute-start(bf16[64,512]{1,0:T(8,128)(2,1)S(1)} %shard_map.80), channel_id=1, source_target_pairs={{160,0},{128,32},{224,64},{192,96},{32,128},{0,160},{96,192},{64,2... | collective-permute-start | bytes 196616 | tf_op jit(solution)/shard_map/ppermute | solution.py:177
  103.3 1.2 %collective-permute-start.8 = (bf16[64,512]{1,0:T(8,128)(2,1)S(1)}, bf16[64,512]{1,0:T(8,128)(2,1)S(1)}, u32[]{:S(2)}, u32[]{:S(2)}) collective-permute-start(bf16[64,512]{1,0:T(8,128)(2,1)S(1)} %shard_map.81), channel_id=1, source_target_pairs={{64,0},{224,32},{128,64},{32,96},{192,128},{96,160},{0,192},{160,2... | collective-permute-start | bytes 196616 | tf_op jit(solution)/shard_map/ppermute | solution.py:177
  104.5 0.0 collective-permute-done.9
  104.5 3.5 %collective-permute-done.7 = bf16[64,512]{1,0:T(8,128)(2,1)S(1)} collective-permute-done((bf16[64,512]{1,0:T(8,128)(2,1)S(1)}, bf16[64,512]{1,0:T(8,128)(2,1)S(1)}, u32[]{:S(2)}, u32[]{:S(2)}) %collective-permute-start.7) | collective-permute-done | bytes 65568 | tf_op jit(solution)/shard_map/ppermute | solution.py:177
  108.0 2.3 %collective-permute-done.8 = bf16[64,512]{1,0:T(8,128)(2,1)S(1)} collective-permute-done((bf16[64,512]{1,0:T(8,128)(2,1)S(1)}, bf16[64,512]{1,0:T(8,128)(2,1)S(1)}, u32[]{:S(2)}, u32[]{:S(2)}) %collective-permute-start.8) | collective-permute-done | bytes 65568 | tf_op jit(solution)/shard_map/ppermute | solution.py:177
  110.2 0.7 add_convert_fusion
Async XLA Ops:
  0.0 1.5 %collective-permute-start = (bf16[64,512]{1,0:T(8,128)(2,1)}, bf16[64,512]{1,0:T(8,128)(2,1)S(1)}, u32[]{:S(2)}, u32[]{:S(2)}) collective-permute-start(bf16[64,512]{1,0:T(8,128)(2,1)} %own_ref.1), channel_id=1, source_target_pairs={{0,1},{1,0},{2,3},{3,2},{4,5},{5,4},{6,7},{7,6},{8,9},{9,8},{10,11... | collective-permute-start | bytes 196616 | tf_op jit(solution)/shard_map/ppermute | solution.py:172
  1.5 0.9 copy-start.4
  2.5 8.4 %collective-permute-start.3 = (bf16[72,512]{1,0:T(8,128)(2,1)S(1)}, bf16[72,512]{1,0:T(8,128)(2,1)S(1)}, u32[]{:S(2)}, u32[]{:S(2)}) collective-permute-start(bf16[72,512]{1,0:T(8,128)(2,1)S(1)} %shard_map.74.own_ref), channel_id=1, source_target_pairs={{0,224},{32,64},{64,32},{96,128},{128,96},{160,192},{192,160},{224... | collective-permute-start | bytes 221192 | tf_op jit(solution)/shard_map/ppermute | solution.py:177
  4.5 7.1 %collective-permute-start.2 = (bf16[72,512]{1,0:T(8,128)(2,1)S(1)}, bf16[72,512]{1,0:T(8,128)(2,1)S(1)}, u32[]{:S(2)}, u32[]{:S(2)}) collective-permute-start(bf16[72,512]{1,0:T(8,128)(2,1)S(1)} %shard_map.74.own_ref), channel_id=1, source_target_pairs={{0,64},{32,224},{64,128},{96,32},{128,192},{160,96},{192,0},{224,1... | collective-permute-start | bytes 221192 | tf_op jit(solution)/shard_map/ppermute | solution.py:177
  8.1 10.0 %collective-permute-start.1 = (bf16[72,512]{1,0:T(8,128)(2,1)S(1)}, bf16[72,512]{1,0:T(8,128)(2,1)S(1)}, u32[]{:S(2)}, u32[]{:S(2)}) collective-permute-start(bf16[72,512]{1,0:T(8,128)(2,1)S(1)} %shard_map.74.own_ref), channel_id=1, source_target_pairs={{0,160},{32,128},{64,224},{96,192},{128,32},{160,0},{192,96},{224,... | collective-permute-start | bytes 221192 | tf_op jit(solution)/shard_map/ppermute | solution.py:177
  18.9 1.3 %copy-start = (bf16[32,64,512]{2,1,0:T(8,128)(2,1)}, bf16[32,64,512]{2,1,0:T(8,128)(2,1)S(1)}, u32[]{:S(2)}) copy-start(bf16[32,64,512]{2,1,0:T(8,128)(2,1)S(1)} %get-tuple-element.12) | copy-start | bytes 6291460
  20.2 9.2 %copy-start.1 = (bf16[2,1024,256]{2,1,0:T(8,128)(2,1)S(1)}, bf16[2,1024,256]{2,1,0:T(8,128)(2,1)}, u32[]{:S(2)}) copy-start(bf16[2,1024,256]{2,1,0:T(8,128)(2,1)} %gate_ref.1) | copy-start | bytes 3145732
  20.2 36.4 %all-to-all-start = ((bf16[64,32,512]{2,1,0:T(8,128)(2,1)}), bf16[64,32,512]{2,1,0:T(8,128)(2,1)S(1)}, u32[]{:S(2)}, u32[]{:S(2)}) async-start(bf16[64,32,512]{2,1,0:T(8,128)(2,1)} %bitcast.14), calls=%async_computation | async-start | bytes 4194304 | tf_op jit(solution)/shard_map/all_to_all | solution.py:180
  29.4 29.8 %collective-permute-start.4 = (bf16[2,1024,256]{2,1,0:T(8,128)(2,1)S(1)}, bf16[2,1024,256]{2,1,0:T(8,128)(2,1)}, u32[]{:S(2)}, u32[]{:S(2)}) collective-permute-start(bf16[2,1024,256]{2,1,0:T(8,128)(2,1)S(1)} %copy-done.1), channel_id=1, source_target_pairs={{0,1},{1,0},{2,3},{3,2},{4,5},{5,4},{6,7},{7,6},{8,9},{9,8},{10,11... | collective-permute-start | bytes 3145736 | tf_op jit(solution)/shard_map/ppermute | solution.py:172
  29.6 29.6 %collective-permute-start.5 = (bf16[2,1024,256]{2,1,0:T(8,128)(2,1)}, bf16[2,1024,256]{2,1,0:T(8,128)(2,1)}, u32[]{:S(2)}, u32[]{:S(2)}) collective-permute-start(bf16[2,1024,256]{2,1,0:T(8,128)(2,1)} %up_ref.1), channel_id=1, source_target_pairs={{0,1},{1,0},{2,3},{3,2},{4,5},{5,4},{6,7},{7,6},{8,9},{9,8},{10,11... | collective-permute-start | bytes 3145736 | tf_op jit(solution)/shard_map/ppermute | solution.py:172
  30.0 29.2 %collective-permute-start.6 = (bf16[2,512,512]{2,1,0:T(8,128)(2,1)}, bf16[2,512,512]{2,1,0:T(8,128)(2,1)}, u32[]{:S(2)}, u32[]{:S(2)}) collective-permute-start(bf16[2,512,512]{2,1,0:T(8,128)(2,1)} %down_ref.1), channel_id=1, source_target_pairs={{0,1},{1,0},{2,3},{3,2},{4,5},{5,4},{6,7},{7,6},{8,9},{9,8},{10,11... | collective-permute-start | bytes 3145736 | tf_op jit(solution)/shard_map/ppermute | solution.py:172
  56.7 1.2 %copy-start.2 = (bf16[2,1024,256]{2,1,0:T(8,128)(2,1)S(1)}, bf16[2,1024,256]{2,1,0:T(8,128)(2,1)}, u32[]{:S(2)}) copy-start(bf16[2,1024,256]{2,1,0:T(8,128)(2,1)} %up_ref.1) | copy-start | bytes 3145732
  57.9 1.3 %copy-start.3 = (bf16[2,512,512]{2,1,0:T(8,128)(2,1)S(1)}, bf16[2,512,512]{2,1,0:T(8,128)(2,1)}, u32[]{:S(2)}) copy-start(bf16[2,512,512]{2,1,0:T(8,128)(2,1)} %down_ref.1) | copy-start | bytes 3145732
  99.5 5.0 %collective-permute-start.9 = (bf16[64,512]{1,0:T(8,128)(2,1)S(1)}, bf16[64,512]{1,0:T(8,128)(2,1)S(1)}, u32[]{:S(2)}, u32[]{:S(2)}) collective-permute-start(bf16[64,512]{1,0:T(8,128)(2,1)S(1)} %get-tuple-element.16), channel_id=1, source_target_pairs={{224,0},{64,32},{32,64},{128,96},{96,128},{192,160},{160,192},{0,2... | collective-permute-start | bytes 196616 | tf_op jit(solution)/shard_map/ppermute | solution.py:177
  99.9 8.1 %collective-permute-start.7 = (bf16[64,512]{1,0:T(8,128)(2,1)S(1)}, bf16[64,512]{1,0:T(8,128)(2,1)S(1)}, u32[]{:S(2)}, u32[]{:S(2)}) collective-permute-start(bf16[64,512]{1,0:T(8,128)(2,1)S(1)} %shard_map.80), channel_id=1, source_target_pairs={{160,0},{128,32},{224,64},{192,96},{32,128},{0,160},{96,192},{64,2... | collective-permute-start | bytes 196616 | tf_op jit(solution)/shard_map/ppermute | solution.py:177
  103.3 6.9 %collective-permute-start.8 = (bf16[64,512]{1,0:T(8,128)(2,1)S(1)}, bf16[64,512]{1,0:T(8,128)(2,1)S(1)}, u32[]{:S(2)}, u32[]{:S(2)}) collective-permute-start(bf16[64,512]{1,0:T(8,128)(2,1)S(1)} %shard_map.81), channel_id=1, source_target_pairs={{64,0},{224,32},{128,64},{32,96},{192,128},{96,160},{0,192},{160,2... | collective-permute-start | bytes 196616 | tf_op jit(solution)/shard_map/ppermute | solution.py:177
